TPU v7x, 32 devices: a whole 2x2x4 slice. The times are simulated.
32 devices in a mesh: ep: 8 (over z, core), tp: 4 (over y, x).
Axes of the slice: x: 2, y: 2, z: 4, core: 2. Of those that a mesh axis runs over, the one named last changes fastest.
Arguments:
- mixer_input: bfloat16 [1024, 2048], P('ep'), may hold values from -6 to 6
- mixer_gain: float32 [2048], replicated, may hold values from 0.1 to 1.9
- glu_value_weight: bfloat16 [512, 2048], P('tp'), may hold values from -0.125 to 0.125
- glu_gate_weight: bfloat16 [512, 2048], P('tp'), may hold values from -0.125 to 0.125
- conv_taps: float32 [512, 31], P('tp'), may hold values from -1 to 1
- conv_bias: float32 [512], P('tp'), may hold values from -3 to 3
- channel_gain: float32 [512], replicated, may hold values from 0.1 to 1.9
- channel_shift: float32 [512], replicated, may hold values from -3 to 3
- mixer_out_weight: bfloat16 [512, 2048], P(None, 'tp'), may hold values from -0.25 to 0.25
- expert_input: bfloat16 [2048, 2048], P('ep'), may hold values from -6 to 6
- expert_gain: float32 [2048], replicated, may hold values from 0.1 to 1.9
- routes: int32 [2048, 2], P('ep'), may hold values from 0 to 7, all different within a row; in each aligned block of 256 rows (0 to 255, 256 to 511, ...) at most 96 rows name the same one
- route_logits: float32 [2048, 2], P('ep'), may hold values from -8 to 8
- gate_weight: bfloat16 [8, 2048, 4096], P('ep', None, 'tp'), may hold values from -0.125 to 0.125
- up_weight: bfloat16 [8, 2048, 4096], P('ep', None, 'tp'), may hold values from -0.125 to 0.125
- down_weight: bfloat16 [8, 4096, 2048], P('ep', 'tp'), may hold values from -0.09375 to 0.09375
Outputs:
- mixer_output: bfloat16 [1024, 2048], P('ep', 'tp')
- expert_output: bfloat16 [2048, 2048], P('ep', 'tp')
Inputs may be any that keep to these rules, and one draw needn't show every extreme that they name: `routes`: the 2 entries of a row differ. Among the rows of one index of ep, no expert is named by more than 96 rows, a bound that some block reaches.
All inputs are finite; a program needn't handle non-finite values.
Results may differ from a plain program's by a relative error of at most 0.015.
Values may be sent and summed in bfloat16 or wider, within the bound.
A program may use at most 64 MiB of HBM per device.

v0:
```python
import functools

import jax
import jax.numpy as jnp
from jax import lax
from jax.experimental import pallas as pl
from jax.experimental.pallas import tpu as pltpu
from jax.sharding import PartitionSpec as P

norm_eps = 1e-06
MESH = pl.DeviceIdType.MESH
f32 = jnp.float32
bf16 = jnp.bfloat16


def step_kernel(
    n_ep, n_tp, cap,
    x_ref, gain_ref, routes_ref, routes_t_ref, logits_ref, gate_hbm, up_hbm, down_hbm,
    mix_gain_ref, taps_ref, bias_ref, chan_gain_ref, chan_shift_ref,
    mix_hbm, value_hbm, glu_gate_hbm, mix_out_hbm,
    out_ref, mix_out_ref,
    gate_w, up_w, down_w, normed, out_part, out_pair, xin, hidden, part, own_part, got, summed, ret,
    w_sem, z_send, z_recv, ag_send, ag_recv, rs_send, rs_recv, y_send, y_recv,
    mix_in, value_w, glu_gate_w, mix_out_w, gated, tail, padded, conv_own, channels,
    tail_sem, c_send, c_recv,
):
    e = lax.axis_index("ep")
    t = lax.axis_index("tp")
    n_z = n_ep // 2
    z = e // 2
    c = e % 2
    mate = e + 1 - 2 * c
    width = out_part.shape[1]
    rows, feat = x_ref.shape
    pair = 2 * cap
    slots = n_ep * cap
    peers = n_tp - 1

    weight_copies = [
        pltpu.make_async_copy(gate_hbm.at[0], gate_w, w_sem.at[0]),
        pltpu.make_async_copy(up_hbm.at[0], up_w, w_sem.at[1]),
        pltpu.make_async_copy(down_hbm.at[0], down_w, w_sem.at[2]),
    ]
    mix_copies = [
        pltpu.make_async_copy(mix_hbm, mix_in, w_sem.at[3]),
        pltpu.make_async_copy(value_hbm, value_w, w_sem.at[4]),
        pltpu.make_async_copy(glu_gate_hbm, glu_gate_w, w_sem.at[5]),
        pltpu.make_async_copy(mix_out_hbm, mix_out_w, w_sem.at[6]),
    ]
    for copy in mix_copies[:3] + weight_copies + mix_copies[3:]:
        copy.start()

    barrier = pltpu.get_barrier_semaphore()
    for o in range(1, n_ep):
        pl.semaphore_signal(barrier, inc=1, device_id=((e + o) % n_ep, t), device_id_type=MESH)
    for o in range(1, n_tp):
        pl.semaphore_signal(barrier, inc=1, device_id=(e, (t + o) % n_tp), device_id_type=MESH)

    def rows_of(index, count):
        return pl.ds(pl.multiple_of(index * count, count), count)

    def cols_of(index, count):
        return pl.ds(pl.multiple_of(index * count, count), count)

    values = x_ref[...].astype(f32)
    scale = lax.rsqrt(jnp.mean(values * values, axis=-1, keepdims=True) + norm_eps)
    normed[...] = (values * scale * gain_ref[...]).astype(bf16)

    lanes = lax.broadcasted_iota(jnp.int32, (rows, 128), 1)
    m0 = (lanes == routes_ref[:, 0:1]).astype(f32)
    m1 = (lanes == routes_ref[:, 1:2]).astype(f32)
    ri = lax.broadcasted_iota(jnp.int32, (rows, rows), 0)
    ci = lax.broadcasted_iota(jnp.int32, (rows, rows), 1)
    lower = (ci < ri).astype(f32).astype(bf16)
    upper = (ri < ci).astype(f32).astype(bf16)
    count = jnp.dot(lower, (m0 + m1).astype(bf16), preferred_element_type=f32)
    base = count + (lanes * cap).astype(f32)
    place0 = jnp.sum(base * m0, axis=1, keepdims=True).astype(jnp.int32)
    place1 = jnp.sum(base * m1, axis=1, keepdims=True).astype(jnp.int32)
    subs = lax.broadcasted_iota(jnp.int32, (128, rows), 0)
    t0 = (subs == routes_t_ref[0:1, :]).astype(f32)
    t1 = (subs == routes_t_ref[1:2, :]).astype(f32)
    count_t = jnp.dot((t0 + t1).astype(bf16), upper, preferred_element_type=f32)
    base_t = count_t + (subs * cap).astype(f32)
    row0 = jnp.sum(base_t * t0, axis=0, keepdims=True).astype(jnp.int32)
    row1 = jnp.sum(base_t * t1, axis=0, keepdims=True).astype(jnp.int32)

    def pick(first, size):
        at = lax.broadcasted_iota(jnp.int32, (size, rows), 0) + first
        return ((at == row0) | (at == row1)).astype(f32).astype(bf16)

    out_part[...] = jnp.dot(
        pick(0, slots), normed[:, cols_of(t, width)], preferred_element_type=f32
    ).astype(bf16)

    pl.semaphore_wait(barrier, n_ep - 1 + peers)

    z_copies = []
    for k in range(1, n_z):
        for cc in range(2):
            dest = ((z + k) % n_z) * 2 + cc
            copy = pltpu.make_async_remote_copy(
                src_ref=out_part.at[rows_of(dest, cap), :],
                dst_ref=xin.at[rows_of(e, cap), cols_of(t, width)],
                send_sem=z_send.at[2 * k + cc],
                recv_sem=z_recv.at[2 * k + c],
                device_id=(dest, t),
                device_id_type=MESH,
            )
            copy.start()
            z_copies.append(copy)

    out_pair[...] = jnp.dot(
        pick(mate * cap, cap), normed[...], preferred_element_type=f32
    ).astype(bf16)
    mate_copy = pltpu.make_async_remote_copy(
        src_ref=out_pair,
        dst_ref=xin.at[rows_of(e, cap), :],
        send_sem=z_send.at[0],
        recv_sem=z_recv.at[0],
        device_id=(mate, t),
        device_id_type=MESH,
    )
    mate_copy.start()
    xin[rows_of(e, cap), :] = jnp.dot(
        pick(e * cap, cap), normed[...], preferred_element_type=f32
    ).astype(bf16)

    def source_chip(k):
        return (z + n_z - k) % n_z

    ag_copies = []

    def gather(k):
        chip = source_chip(k)
        for cc in range(2):
            block = xin.at[rows_of(chip * 2 + cc, cap), cols_of(t, width)]
            pltpu.make_async_remote_copy(
                src_ref=block, dst_ref=block, send_sem=z_send.at[2 * k + cc],
                recv_sem=z_recv.at[2 * k + cc], device_id=(mate, t), device_id_type=MESH,
            ).wait_recv()
        block = xin.at[rows_of(chip, pair), cols_of(t, width)]
        for o in range(1, n_tp):
            copy = pltpu.make_async_remote_copy(
                src_ref=block, dst_ref=block, send_sem=ag_send.at[k * peers + o - 1],
                recv_sem=ag_recv.at[k * peers + o - 1],
                device_id=(e, (t + o) % n_tp), device_id_type=MESH,
            )
            copy.start()
            ag_copies.append(copy)

    def gathered(k):
        chip = source_chip(k)
        for o in range(1, n_tp):
            block = xin.at[rows_of(chip, pair), cols_of((t + n_tp - o) % n_tp, width)]
            pltpu.make_async_remote_copy(
                src_ref=block, dst_ref=block, send_sem=ag_send.at[k * peers + o - 1],
                recv_sem=ag_recv.at[k * peers + o - 1],
                device_id=(mate, t), device_id_type=MESH,
            ).wait_recv()

    units = gate_w.shape[1]
    tile = min(units, 256)
    rs_copies = []
    y_copies = []

    def up_half(k):
        here = rows_of(source_chip(k), pair)

        def one(j, carry):
            cols = cols_of(j, tile)
            rows_in = xin[here, :]
            g = jnp.dot(rows_in, gate_w[:, cols], preferred_element_type=f32)
            u = jnp.dot(rows_in, up_w[:, cols], preferred_element_type=f32)
            hidden[:, cols] = (g * jax.nn.sigmoid(g) * u).astype(bf16)
            return carry

        lax.fori_loop(0, units // tile, one, 0)

    def down_half(k):
        for o in range(1, n_tp):
            peer = (t + o) % n_tp
            at = k * peers + o - 1
            part[at] = jnp.dot(
                hidden[...], down_w[:, cols_of(peer, width)], preferred_element_type=f32
            ).astype(bf16)
            copy = pltpu.make_async_remote_copy(
                src_ref=part.at[at], dst_ref=got.at[at], send_sem=rs_send.at[at],
                recv_sem=rs_recv.at[at], device_id=(e, peer), device_id_type=MESH,
            )
            copy.start()
            rs_copies.append(copy)
        own_part[k] = jnp.dot(
            hidden[...], down_w[:, cols_of(t, width)], preferred_element_type=f32
        ).astype(bf16)

    def finish(k):
        chip = source_chip(k)
        total = own_part[k].astype(f32)
        for o in range(1, n_tp):
            at = k * peers + o - 1
            pltpu.make_async_remote_copy(
                src_ref=part.at[at], dst_ref=got.at[at], send_sem=rs_send.at[at],
                recv_sem=rs_recv.at[at], device_id=(mate, t), device_id_type=MESH,
            ).wait_recv()
            total = total + got[at].astype(f32)
        summed[k] = total.astype(bf16)
        if k == 0:
            copy = pltpu.make_async_remote_copy(
                src_ref=summed.at[0, rows_of(1 - c, cap), :], dst_ref=ret.at[rows_of(e, cap), :],
                send_sem=y_send.at[0], recv_sem=y_recv.at[0],
                device_id=(mate, t), device_id_type=MESH,
            )
            copy.start()
            y_copies.append(copy)
            ret[rows_of(e, cap), :] = summed[0, rows_of(c, cap), :]
            return
        for cc in range(2):
            copy = pltpu.make_async_remote_copy(
                src_ref=summed.at[k, pl.ds(cc * cap, cap), :], dst_ref=ret.at[rows_of(e, cap), :],
                send_sem=y_send.at[2 * k + cc], recv_sem=y_recv.at[2 * k + c],
                device_id=(chip * 2 + cc, t), device_id_type=MESH,
            )
            copy.start()
            y_copies.append(copy)

    taken, chans = gated.shape
    keep = tail.shape[0]
    reach = taps_ref.shape[0] - 1
    conv_copies = []

    def tail_copy():
        return pltpu.make_async_remote_copy(
            src_ref=gated.at[pl.ds(taken - keep, keep), :], dst_ref=tail,
            send_sem=tail_sem.at[0], recv_sem=tail_sem.at[1],
            device_id=((e + 1) % n_ep, t), device_id_type=MESH,
        )

    def glu():
        for copy in mix_copies[:3]:
            copy.wait()
        mixed = mix_in[...].astype(f32)
        inv = lax.rsqrt(jnp.mean(mixed * mixed, axis=-1, keepdims=True) + norm_eps)
        normed_a = (mixed * inv * mix_gain_ref[...]).astype(bf16)
        contract = (((1,), (1,)), ((), ()))
        value = lax.dot_general(normed_a, value_w[...], contract, preferred_element_type=f32)
        gate = lax.dot_general(normed_a, glu_gate_w[...], contract, preferred_element_type=f32)
        gated[...] = (value * jax.nn.sigmoid(gate)).astype(bf16)
        copy = tail_copy()
        copy.start()
        conv_copies.append(copy)

    def convolve():
        tail_copy().wait_recv()
        before = tail[...].astype(f32)
        padded[pl.ds(0, keep), :] = jnp.where(e > 0, before, jnp.zeros_like(before))
        padded[pl.ds(keep, taken), :] = gated[...].astype(f32)
        total = jnp.zeros((taken, chans), f32)
        for offset in range(reach + 1):
            shift = keep - reach + offset
            total = total + padded[pl.ds(shift, taken), :] * taps_ref[offset : offset + 1, :]
        done = (total + bias_ref[...]).astype(bf16)
        conv_own[...] = done
        channels[t] = done
        for o in range(1, n_tp):
            copy = pltpu.make_async_remote_copy(
                src_ref=conv_own, dst_ref=channels.at[t],
                send_sem=c_send.at[o - 1], recv_sem=c_recv.at[o - 1],
                device_id=(e, (t + o) % n_tp), device_id_type=MESH,
            )
            copy.start()
            conv_copies.append(copy)

    def mixer_end():
        for o in range(1, n_tp):
            pltpu.make_async_remote_copy(
                src_ref=conv_own, dst_ref=channels.at[(t + n_tp - o) % n_tp],
                send_sem=c_send.at[o - 1], recv_sem=c_recv.at[o - 1],
                device_id=(mate, t), device_id_type=MESH,
            ).wait_recv()
        mix_copies[3].wait()
        chan_values = jnp.concatenate([channels[i].astype(f32) for i in range(n_tp)], axis=1)
        centered = chan_values - jnp.mean(chan_values, axis=1, keepdims=True)
        variance = jnp.mean(centered * centered, axis=1, keepdims=True)
        shaped = (
            centered * lax.rsqrt(variance + norm_eps) * chan_gain_ref[...] + chan_shift_ref[...]
        )
        activated = (shaped * jax.nn.sigmoid(shaped)).astype(bf16)
        mix_out_ref[...] = jnp.dot(
            activated, mix_out_w[...], preferred_element_type=f32
        ).astype(bf16)

    glu()
    if n_z > 1:
        gather(1)
    mate_block = xin.at[rows_of(mate, cap), :]
    pltpu.make_async_remote_copy(
        src_ref=mate_block, dst_ref=mate_block, send_sem=z_send.at[0], recv_sem=z_recv.at[0],
        device_id=(mate, t), device_id_type=MESH,
    ).wait_recv()
    weight_copies[0].wait()
    weight_copies[1].wait()
    for k in range(n_z):
        if k > 0:
            gathered(k)
        up_half(k)
        if k == 0:
            weight_copies[2].wait()
        if k + 2 < n_z:
            gather(k + 2)
        down_half(k)
        if k == 0:
            convolve()
        if k > 0:
            finish(k - 1)
        if k == 1 or n_z == 1:
            mixer_end()
    finish(n_z - 1)

    block = ret.at[rows_of(mate, cap), :]
    pltpu.make_async_remote_copy(
        src_ref=block, dst_ref=block, send_sem=y_send.at[0], recv_sem=y_recv.at[0],
        device_id=(mate, t), device_id_type=MESH,
    ).wait_recv()
    for k in range(1, n_z):
        for cc in range(2):
            block = ret.at[rows_of(((z + k) % n_z) * 2 + cc, cap), :]
            pltpu.make_async_remote_copy(
                src_ref=block, dst_ref=block, send_sem=y_send.at[2 * k + cc],
                recv_sem=y_recv.at[2 * k + cc], device_id=(mate, t), device_id_type=MESH,
            ).wait_recv()
    at = lax.broadcasted_iota(jnp.int32, (rows, slots), 1)
    l0 = logits_ref[:, 0:1]
    l1 = logits_ref[:, 1:2]
    first = jnp.dot(
        (at == place0).astype(f32).astype(bf16), ret[...], preferred_element_type=f32
    )
    second = jnp.dot(
        (at == place1).astype(f32).astype(bf16), ret[...], preferred_element_type=f32
    )
    out_ref[...] = (
        first * jax.nn.sigmoid(l0 - l1) + second * jax.nn.sigmoid(l1 - l0)
    ).astype(bf16)
    for copy in [mate_copy] + z_copies + ag_copies + rs_copies + y_copies + conv_copies:
        copy.wait_send()


def on_device(
    mixer_input, mixer_gain, glu_value_weight, glu_gate_weight, conv_taps, conv_bias,
    channel_gain, channel_shift, mixer_out_weight, expert_input, expert_gain, routes,
    route_logits, gate_weight, up_weight, down_weight,
):
    n_ep, n_tp = lax.axis_size("ep"), lax.axis_size("tp")
    rows, feat = expert_input.shape
    cap = 3 * rows // n_ep
    cap = -(-cap // 16) * 16
    units = gate_weight.shape[2]
    width = feat // n_tp
    n_z, peers, pair, slots = n_ep // 2, n_tp - 1, 2 * cap, n_ep * cap
    taken, chans, taps = mixer_input.shape[0], conv_taps.shape[0], conv_taps.shape[1]
    keep = -(-(taps - 1) // 16) * 16
    vmem = pl.BlockSpec(memory_space=pltpu.VMEM)
    hbm = pl.BlockSpec(memory_space=pl.ANY)
    dma = pltpu.SemaphoreType.DMA
    expert_output, mixer_output = pl.pallas_call(
        functools.partial(step_kernel, n_ep, n_tp, cap),
        out_shape=(
            jax.ShapeDtypeStruct((rows, width), bf16),
            jax.ShapeDtypeStruct((taken, mixer_out_weight.shape[1]), bf16),
        ),
        in_specs=[vmem] * 5 + [hbm] * 3 + [vmem] * 5 + [hbm] * 4,
        out_specs=(vmem, vmem),
        scratch_shapes=[
            pltpu.VMEM((feat, units), bf16),
            pltpu.VMEM((feat, units), bf16),
            pltpu.VMEM((units, feat), bf16),
            pltpu.VMEM((rows, feat), bf16),
            pltpu.VMEM((slots, width), bf16),
            pltpu.VMEM((cap, feat), bf16),
            pltpu.VMEM((slots, feat), bf16),
            pltpu.VMEM((pair, units), bf16),
            pltpu.VMEM((n_z * peers, pair, width), bf16),
            pltpu.VMEM((n_z, pair, width), bf16),
            pltpu.VMEM((n_z * peers, pair, width), bf16),
            pltpu.VMEM((n_z, pair, width), bf16),
            pltpu.VMEM((slots, width), bf16),
            dma((7,)),
            dma((n_ep,)),
            dma((n_ep,)),
            dma((n_z * peers,)),
            dma((n_z * peers,)),
            dma((n_z * peers,)),
            dma((n_z * peers,)),
            dma((n_ep,)),
            dma((n_ep,)),
            pltpu.VMEM(mixer_input.shape, bf16),
            pltpu.VMEM(glu_value_weight.shape, bf16),
            pltpu.VMEM(glu_gate_weight.shape, bf16),
            pltpu.VMEM(mixer_out_weight.shape, bf16),
            pltpu.VMEM((taken, chans), bf16),
            pltpu.VMEM((keep, chans), bf16),
            pltpu.VMEM((keep + taken, chans), f32),
            pltpu.VMEM((taken, chans), bf16),
            pltpu.VMEM((n_tp, taken, chans), bf16),
            dma((2,)),
            dma((peers,)),
            dma((peers,)),
        ],
        compiler_params=pltpu.CompilerParams(
            collective_id=0, has_side_effects=True, vmem_limit_bytes=48 * 1024 * 1024
        ),
        cost_estimate=pl.CostEstimate(
            flops=6 * slots * feat * units, bytes_accessed=6 * feat * units, transcendentals=0
        ),
    )(
        expert_input, expert_gain[None, :], routes, routes.T, route_logits,
        gate_weight, up_weight, down_weight,
        mixer_gain[None, :], conv_taps.T, conv_bias[None, :], channel_gain[None, :],
        channel_shift[None, :], mixer_input, glu_value_weight, glu_gate_weight, mixer_out_weight,
    )
    return (mixer_output, expert_output)


def solution(mesh):
    in_specs = (
        P("ep", None),
        P(),
        P("tp", None),
        P("tp", None),
        P("tp", None),
        P("tp"),
        P(),
        P(),
        P(None, "tp"),
        P("ep", None),
        P(),
        P("ep", None),
        P("ep", None),
        P("ep", None, "tp"),
        P("ep", None, "tp"),
        P("ep", "tp", None),
    )
    out_specs = (P("ep", "tp"), P("ep", "tp"))
    return jax.shard_map(
        on_device, mesh=mesh, in_specs=in_specs, out_specs=out_specs, check_vma=False
    )
```

profile of v0, /device:TPU:1, one launch (start us, length us, event | category | flops | bytes accessed | tf_op | source)
XLA Modules:
  0.0 99.3 jit_solution(7407766748162911397)
XLA Ops:
  0.6 0.8 copy.19.logits_ref
  1.4 0.8 copy.18.routes_ref
  2.3 0.0 copy-start
  2.3 0.7 copy-done
  3.0 0.0 copy-start.1
  3.0 1.2 %copy-done.1 = bf16[256,2048]{1,0:T(8,128)(2,1)S(1)} copy-done((bf16[256,2048]{1,0:T(8,128)(2,1)S(1)}, bf16[256,2048]{1,0:T(8,128)(2,1)}, u32[]{:S(2)}) %copy-start.1) | copy-done | bytes 1048600
  4.2 0.0 copy-start.2
  4.2 1.0 %copy-done.2 = bf16[128,2048]{1,0:T(8,128)(2,1)S(1)} copy-done((bf16[128,2048]{1,0:T(8,128)(2,1)S(1)}, bf16[128,2048]{1,0:T(8,128)(2,1)}, u32[]{:S(2)}) %copy-start.2) | copy-done | bytes 524312
  5.2 0.0 copy-start.3
  5.2 1.0 %copy-done.3 = bf16[128,2048]{1,0:T(8,128)(2,1)S(1)} copy-done((bf16[128,2048]{1,0:T(8,128)(2,1)S(1)}, bf16[128,2048]{1,0:T(8,128)(2,1)}, u32[]{:S(2)}) %copy-start.3) | copy-done | bytes 524312
  6.3 0.0 copy-start.4
  6.3 1.0 %copy-done.4 = bf16[128,2048]{1,0:T(8,128)(2,1)S(1)} copy-done((bf16[128,2048]{1,0:T(8,128)(2,1)S(1)}, bf16[128,2048]{1,0:T(8,128)(2,1)}, u32[]{:S(2)}) %copy-start.4) | copy-done | bytes 524312
  7.3 0.0 copy-start.5
  7.3 1.0 %copy-done.5 = bf16[512,512]{1,0:T(8,128)(2,1)S(1)} copy-done((bf16[512,512]{1,0:T(8,128)(2,1)S(1)}, bf16[512,512]{1,0:T(8,128)(2,1)}, u32[]{:S(2)}) %copy-start.5) | copy-done | bytes 524312
  8.3 0.0 copy-start.6
  8.4 0.7 copy-done.6
  9.1 0.0 copy-start.7
  9.1 0.7 copy-done.7
  9.8 0.0 copy-start.8
  9.8 0.7 copy-done.8
  10.5 0.0 copy-start.9
  10.5 0.7 copy-done.9
  11.1 0.0 copy-start.10
  11.1 0.7 copy-done.10
  11.8 0.0 copy-start.11
  11.8 0.7 copy-done.11
  12.5 85.5 %shard_map.167 = (bf16[256,512]{1,0:T(8,128)(2,1)S(1)}, bf16[128,512]{1,0:T(8,128)(2,1)S(1)}) custom-call(bf16[256,2048]{1,0:T(8,128)(2,1)S(1)} %copy-done.1, f32[1,2048]{1,0:T(1,128)S(1)} %bitcast.9, s32[256,2]{1,0:T(8,128)S(1)} %copy.18.routes_ref, s32[2,256]{1,0:T(2,128)S(1)} %bitcast.7, f32[256,2]{1,0:T(8,128)S(1)} %copy.19.logits_ref, ...), custom_call_target="tpu_custom_call" | custom-call | flops 9663676416 | bytes 12582912 | tf_op jit(solution)/shard_map/pallas_call | solution.py:365
  98.0 0.7 copy.22
  98.6 0.7 copy.23
Async XLA Ops:
  2.3 0.7 copy-start
  3.0 1.2 %copy-start.1 = (bf16[256,2048]{1,0:T(8,128)(2,1)S(1)}, bf16[256,2048]{1,0:T(8,128)(2,1)}, u32[]{:S(2)}) copy-start(bf16[256,2048]{1,0:T(8,128)(2,1)} %x_ref.1) | copy-start | bytes 3145732
  4.2 1.0 %copy-start.2 = (bf16[128,2048]{1,0:T(8,128)(2,1)S(1)}, bf16[128,2048]{1,0:T(8,128)(2,1)}, u32[]{:S(2)}) copy-start(bf16[128,2048]{1,0:T(8,128)(2,1)} %mix_hbm.1) | copy-start | bytes 1572868
  5.2 1.0 %copy-start.3 = (bf16[128,2048]{1,0:T(8,128)(2,1)S(1)}, bf16[128,2048]{1,0:T(8,128)(2,1)}, u32[]{:S(2)}) copy-start(bf16[128,2048]{1,0:T(8,128)(2,1)} %value_hbm.1) | copy-start | bytes 1572868
  6.3 1.0 %copy-start.4 = (bf16[128,2048]{1,0:T(8,128)(2,1)S(1)}, bf16[128,2048]{1,0:T(8,128)(2,1)}, u32[]{:S(2)}) copy-start(bf16[128,2048]{1,0:T(8,128)(2,1)} %glu_gate_hbm.1) | copy-start | bytes 1572868
  7.3 1.0 %copy-start.5 = (bf16[512,512]{1,0:T(8,128)(2,1)S(1)}, bf16[512,512]{1,0:T(8,128)(2,1)}, u32[]{:S(2)}) copy-start(bf16[512,512]{1,0:T(8,128)(2,1)} %mix_out_hbm.1) | copy-start | bytes 1572868
  8.3 0.7 copy-start.6
  9.1 0.7 copy-start.7
  9.8 0.7 copy-start.8
  10.5 0.7 copy-start.9
  11.1 0.7 copy-start.10
  11.8 0.7 copy-start.11
where the time goes:
time: 100 us; the launch traced here: 99.3 us
  Pallas kernels  85.5 us (86%)
  local copies, waits for them, and re-layouts  13.2 us (13%)
    pallas_call x1, Pallas kernels, on_device(): pl.pallas_call(functools.partial(step_kernel, n_ep, n_tp, cap), out_shape...  85.5 us
    unnamed x28, local copies, waits for them, and re-layouts  13.2 us

commit v1 on v0

--- a/solution.py
+++ b/solution.py
@@ -345,7 +345,481 @@
         copy.wait_send()
 
 
-def on_device(
+def paired_kernel(
+    n_ep, n_tp, cap,
+    x_hbm, gain_hbm, routes_hbm, logits_hbm, gate_hbm, up_hbm, down_hbm,
+    mix_gain_hbm, taps_hbm, bias_hbm, chan_gain_hbm, chan_shift_hbm,
+    mix_hbm, value_hbm, glu_gate_hbm, mix_out_hbm,
+    out_ref, mix_out_ref,
+    x_in, gain_in, routes_in, logits_in, gate_w, up_w, down_w,
+    mix_gain_in, taps_in, bias_in, chan_gain_in, chan_shift_in,
+    mix_in, value_w, glu_gate_w, mix_out_w,
+    normed, columns, out_part, out_pair, xin, hidden,
+    part_x, part_y, got_x, got_y, held_own, held_x, held_y, pass_x, pass_y, last_x, last_y,
+    summed, ret, acc,
+    load_sem, z_send, z_recv, ag_send, ag_recv, rs_send, rs_recv, y_send, y_recv,
+    gated, tail, padded, conv_own, channels,
+    tail_sem, c_send, c_recv,
+):
+    e = lax.axis_index("ep")
+    t = lax.axis_index("tp")
+    n_z = n_ep // 2
+    z = e // 2
+    c = e % 2
+    mate = e + 1 - 2 * c
+    rows, feat = x_in.shape
+    width = out_part.shape[1]
+    half = width // 2
+    pair = 2 * cap
+    slots = n_ep * cap
+    units = gate_w.shape[1]
+    tile = min(units, 256)
+    tiles = units // tile
+    t_x = t + 1 - 2 * (t % 2)
+    t_y = (t + 2) % 4
+    t_d = 3 - t
+
+    def chip_of(k):
+        return [z, z + 1 - 2 * (z % 2), (z + 2) % 4, 3 - z][k]
+
+    def rows_of(index, count):
+        return pl.ds(pl.multiple_of(index * count, count), count)
+
+    def cols(quarter, first, count):
+        return pl.ds(pl.multiple_of(quarter * width + first, 128), count)
+
+    def load(src, dst, at):
+        return pltpu.make_async_copy(src, dst, load_sem.at[at])
+
+    def weight_tile(j):
+        here = pl.ds(pl.multiple_of(j * tile, tile), tile)
+        return (
+            load(gate_hbm.at[0, :, here], gate_w.at[:, here], 16 + 2 * j),
+            load(up_hbm.at[0, :, here], up_w.at[:, here], 17 + 2 * j),
+        )
+
+    load_routes = load(routes_hbm, routes_in, 0)
+    load_logits = load(logits_hbm, logits_in, 1)
+    load_gain = load(gain_hbm, gain_in, 2)
+    load_x = load(x_hbm, x_in, 3)
+    load_mix = [
+        load(mix_hbm, mix_in, 4), load(mix_gain_hbm, mix_gain_in, 5),
+        load(value_hbm, value_w, 6), load(glu_gate_hbm, glu_gate_w, 7),
+    ]
+    load_conv = [load(taps_hbm, taps_in, 8), load(bias_hbm, bias_in, 9)]
+    load_end = [
+        load(chan_gain_hbm, chan_gain_in, 10), load(chan_shift_hbm, chan_shift_in, 11),
+        load(mix_out_hbm, mix_out_w, 12),
+    ]
+    load_down = load(down_hbm.at[0], down_w, 13)
+    for copy in [load_x, load_gain, load_routes, load_logits] + load_mix + load_conv:
+        copy.start()
+    for j in range(tiles):
+        for copy in weight_tile(j):
+            copy.start()
+    for copy in [load_down] + load_end:
+        copy.start()
+
+    barrier = pltpu.get_barrier_semaphore()
+    for o in range(1, n_ep):
+        pl.semaphore_signal(barrier, inc=1, device_id=((e + o) % n_ep, t), device_id_type=MESH)
+    for o in range(1, n_tp):
+        pl.semaphore_signal(barrier, inc=1, device_id=(e, (t + o) % n_tp), device_id_type=MESH)
+
+    load_routes.wait()
+    ri = lax.broadcasted_iota(jnp.int32, (rows, rows), 0)
+    ci = lax.broadcasted_iota(jnp.int32, (rows, rows), 1)
+    upper = (ri < ci).astype(f32).astype(bf16)
+    subs = lax.broadcasted_iota(jnp.int32, (128, rows), 0)
+    t0 = (subs == routes_in[0:1, :]).astype(f32)
+    t1 = (subs == routes_in[1:2, :]).astype(f32)
+    count_t = jnp.dot((t0 + t1).astype(bf16), upper, preferred_element_type=f32)
+    base_t = count_t + (subs * cap).astype(f32)
+    place0 = jnp.sum(base_t * t0, axis=0, keepdims=True)
+    place1 = jnp.sum(base_t * t1, axis=0, keepdims=True)
+    row0 = place0.astype(jnp.int32)
+    row1 = place1.astype(jnp.int32)
+
+    def pick(first, size):
+        at = lax.broadcasted_iota(jnp.int32, (size, rows), 0) + first
+        return ((at == row0) | (at == row1)).astype(f32).astype(bf16)
+
+    load_x.wait()
+    load_gain.wait()
+    values = x_in[...].astype(f32)
+    scale = lax.rsqrt(jnp.mean(values * values, axis=-1, keepdims=True) + norm_eps)
+    normed[...] = (values * scale * gain_in[...]).astype(bf16)
+    out_part[...] = jnp.dot(
+        pick(0, slots), normed[:, cols(t, 0, width)], preferred_element_type=f32
+    ).astype(bf16)
+
+    pl.semaphore_wait(barrier, n_ep - 1 + n_tp - 1)
+
+    sent = []
+
+    def send(src, dst, send_sem, recv_sem, to):
+        copy = pltpu.make_async_remote_copy(
+            src_ref=src, dst_ref=dst, send_sem=send_sem, recv_sem=recv_sem,
+            device_id=to, device_id_type=MESH,
+        )
+        copy.start()
+        sent.append(copy)
+
+    def arrive(dst, send_sem, recv_sem):
+        pltpu.make_async_remote_copy(
+            src_ref=dst, dst_ref=dst, send_sem=send_sem, recv_sem=recv_sem,
+            device_id=(mate, t), device_id_type=MESH,
+        ).wait_recv()
+
+    for k in range(1, n_z):
+        for cc in range(2):
+            dest = chip_of(k) * 2 + cc
+            send(
+                out_part.at[rows_of(dest, cap), :], xin.at[rows_of(e, cap), cols(t, 0, width)],
+                z_send.at[2 * k + cc], z_recv.at[2 * k + c], (dest, t),
+            )
+
+    out_pair[...] = jnp.dot(
+        pick(mate * cap, cap), normed[...], preferred_element_type=f32
+    ).astype(bf16)
+    send(out_pair, xin.at[rows_of(e, cap), :], z_send.at[0], z_recv.at[0], (mate, t))
+    xin[rows_of(e, cap), :] = jnp.dot(
+        pick(e * cap, cap), normed[...], preferred_element_type=f32
+    ).astype(bf16)
+
+    def routed(k):
+        for cc in range(2):
+            arrive(
+                xin.at[rows_of(chip_of(k) * 2 + cc, cap), cols(t, 0, width)],
+                z_send.at[2 * k + cc], z_recv.at[2 * k + cc],
+            )
+        block = xin.at[rows_of(chip_of(k), pair), cols(t, 0, width)]
+        send(block, block, ag_send.at[k - 1, 0], ag_recv.at[k - 1, 0], (e, t_x))
+        send(block, block, ag_send.at[k - 1, 1], ag_recv.at[k - 1, 1], (e, t_y))
+
+    def relay(k):
+        here = rows_of(chip_of(k), pair)
+        arrive(xin.at[here, cols(t_y, 0, width)], ag_send.at[k - 1, 1], ag_recv.at[k - 1, 1])
+        block = xin.at[here, cols(t_y, 0, half)]
+        send(block, block, ag_send.at[k - 1, 2], ag_recv.at[k - 1, 2], (e, t_x))
+        arrive(xin.at[here, cols(t_x, 0, width)], ag_send.at[k - 1, 0], ag_recv.at[k - 1, 0])
+        block = xin.at[here, cols(t_x, half, half)]
+        send(block, block, ag_send.at[k - 1, 3], ag_recv.at[k - 1, 3], (e, t_y))
+
+    def gathered(k):
+        here = rows_of(chip_of(k), pair)
+        arrive(xin.at[here, cols(t_d, 0, half)], ag_send.at[k - 1, 2], ag_recv.at[k - 1, 2])
+        arrive(xin.at[here, cols(t_d, half, half)], ag_send.at[k - 1, 3], ag_recv.at[k - 1, 3])
+
+    def up_half(k):
+        here = rows_of(chip_of(k), pair)
+
+        def one(j, carry):
+            if k == 0:
+                for copy in weight_tile(j):
+                    copy.wait()
+            at = pl.ds(pl.multiple_of(j * tile, tile), tile)
+            rows_in = xin[here, :]
+            g = jnp.dot(rows_in, gate_w[:, at], preferred_element_type=f32)
+            u = jnp.dot(rows_in, up_w[:, at], preferred_element_type=f32)
+            hidden[k, :, at] = (g * jax.nn.sigmoid(g) * u).astype(bf16)
+            return carry
+
+        lax.fori_loop(0, tiles, one, 0)
+
+    def group(u):
+        if u == 0:
+            return 0, rows_of(1 - c, cap), pl.ds(0, cap)
+        if u == n_z:
+            return 0, rows_of(c, cap), pl.ds(cap, cap)
+        return u, pl.ds(0, pair), pl.ds(0, pair)
+
+    def down_half(u):
+        k, here, at = group(u)
+
+        def product(quarter):
+            return jnp.dot(
+                hidden[k, here, :], down_w[:, cols(quarter, 0, width)],
+                preferred_element_type=f32,
+            ).astype(bf16)
+
+        def give(src, dst, way, to):
+            send(src, dst, rs_send.at[u, way], rs_recv.at[u, way], (e, to))
+
+        far = product(t_d)
+        part_x[k, 1, at, :] = far[:, :half]
+        part_y[k, 1, at, :] = far[:, half:]
+        give(part_x.at[k, 1, at, :], got_x.at[k, 1, at, :], 0, t_x)
+        give(part_y.at[k, 1, at, :], got_y.at[k, 1, at, :], 1, t_y)
+        near = product(t_x)
+        part_x[k, 0, at, :] = near[:, :half]
+        held_x[k, at, :] = near[:, half:]
+        give(part_x.at[k, 0, at, :], got_x.at[k, 0, at, :], 2, t_x)
+        near = product(t_y)
+        part_y[k, 0, at, :] = near[:, half:]
+        held_y[k, at, :] = near[:, :half]
+        give(part_y.at[k, 0, at, :], got_y.at[k, 0, at, :], 3, t_y)
+        held_own[k, at, :] = product(t)
+
+    def pass_on(u):
+        k, here, at = group(u)
+        arrive(got_x.at[k, 1, at, :], rs_send.at[u, 0], rs_recv.at[u, 0])
+        pass_y[k, at, :] = (
+            held_y[k, at, :].astype(f32) + got_x[k, 1, at, :].astype(f32)
+        ).astype(bf16)
+        send(
+            pass_y.at[k, at, :], last_y.at[k, at, :], rs_send.at[u, 4], rs_recv.at[u, 4], (e, t_y)
+        )
+        arrive(got_y.at[k, 1, at, :], rs_send.at[u, 1], rs_recv.at[u, 1])
+        pass_x[k, at, :] = (
+            held_x[k, at, :].astype(f32) + got_y[k, 1, at, :].astype(f32)
+        ).astype(bf16)
+        send(
+            pass_x.at[k, at, :], last_x.at[k, at, :], rs_send.at[u, 5], rs_recv.at[u, 5], (e, t_x)
+        )
+
+    def finish(u):
+        k, here, at = group(u)
+        arrive(got_x.at[k, 0, at, :], rs_send.at[u, 2], rs_recv.at[u, 2])
+        arrive(got_y.at[k, 0, at, :], rs_send.at[u, 3], rs_recv.at[u, 3])
+        arrive(last_y.at[k, at, :], rs_send.at[u, 4], rs_recv.at[u, 4])
+        arrive(last_x.at[k, at, :], rs_send.at[u, 5], rs_recv.at[u, 5])
+        low = (
+            held_own[k, at, :half].astype(f32)
+            + got_x[k, 0, at, :].astype(f32) + last_y[k, at, :].astype(f32)
+        ).astype(bf16)
+        high = (
+            held_own[k, at, half:].astype(f32)
+            + got_y[k, 0, at, :].astype(f32) + last_x[k, at, :].astype(f32)
+        ).astype(bf16)
+        if u == n_z:
+            ret[rows_of(e, cap), :half] = low
+            ret[rows_of(e, cap), half:] = high
+            return
+        summed[k, at, :half] = low
+        summed[k, at, half:] = high
+        if u == 0:
+            send(
+                summed.at[0, pl.ds(0, cap), :], ret.at[rows_of(e, cap), :],
+                y_send.at[0], y_recv.at[0], (mate, t),
+            )
+            return
+        for cc in range(2):
+            send(
+                summed.at[k, pl.ds(cc * cap, cap), :], ret.at[rows_of(e, cap), :],
+                y_send.at[2 * k + cc], y_recv.at[2 * k + c], (chip_of(k) * 2 + cc, t),
+            )
+
+    def weighted(first, size):
+        at = lax.broadcasted_iota(jnp.int32, (rows, size), 1) + first
+        back = ret[rows_of(first // size, size), :]
+        one = jnp.dot(
+            (at == columns[0, :, 0:1].astype(jnp.int32)).astype(f32).astype(bf16), back,
+            preferred_element_type=f32,
+        )
+        two = jnp.dot(
+            (at == columns[1, :, 0:1].astype(jnp.int32)).astype(f32).astype(bf16), back,
+            preferred_element_type=f32,
+        )
+        return one * columns[2, :, 0:1] + two * columns[3, :, 0:1]
+
+    def returned(k):
+        for cc in range(2):
+            arrive(
+                ret.at[rows_of(chip_of(k) * 2 + cc, cap), :],
+                y_send.at[2 * k + cc], y_recv.at[2 * k + cc],
+            )
+        return weighted(chip_of(k) * pair, pair)
+
+    taken, chans = gated.shape
+    keep = tail.shape[0]
+    reach = taps_in.shape[0] - 1
+
+    def tail_refs():
+        return gated.at[pl.ds(taken - keep, keep), :], tail, tail_sem.at[0], tail_sem.at[1]
+
+    def glu():
+        for copy in load_mix:
+            copy.wait()
+        mixed = mix_in[...].astype(f32)
+        inv = lax.rsqrt(jnp.mean(mixed * mixed, axis=-1, keepdims=True) + norm_eps)
+        normed_a = (mixed * inv * mix_gain_in[...]).astype(bf16)
+        contract = (((1,), (1,)), ((), ()))
+        value = lax.dot_general(normed_a, value_w[...], contract, preferred_element_type=f32)
+        gate = lax.dot_general(normed_a, glu_gate_w[...], contract, preferred_element_type=f32)
+        gated[...] = (value * jax.nn.sigmoid(gate)).astype(bf16)
+        send(*tail_refs(), ((e + 1) % n_ep, t))
+
+    def convolve():
+        for copy in load_conv:
+            copy.wait()
+        arrive(tail, tail_sem.at[0], tail_sem.at[1])
+        before = tail[...].astype(f32)
+        padded[pl.ds(0, keep), :] = jnp.where(e > 0, before, jnp.zeros_like(before))
+        padded[pl.ds(keep, taken), :] = gated[...].astype(f32)
+        total = jnp.zeros((taken, chans), f32)
+        for offset in range(reach + 1):
+            shift = keep - reach + offset
+            total = total + padded[pl.ds(shift, taken), :] * taps_in[offset : offset + 1, :]
+        done = (total + bias_in[...]).astype(bf16)
+        conv_own[...] = done
+        channels[t] = done
+        for o in range(1, n_tp):
+            send(
+                conv_own, channels.at[t], c_send.at[o - 1], c_recv.at[o - 1],
+                (e, (t + o) % n_tp),
+            )
+
+    def mixer_end():
+        for o in range(1, n_tp):
+            arrive(channels.at[(t + n_tp - o) % n_tp], c_send.at[o - 1], c_recv.at[o - 1])
+        for copy in load_end:
+            copy.wait()
+        chan_values = jnp.concatenate([channels[i].astype(f32) for i in range(n_tp)], axis=1)
+        centered = chan_values - jnp.mean(chan_values, axis=1, keepdims=True)
+        variance = jnp.mean(centered * centered, axis=1, keepdims=True)
+        shaped = (
+            centered * lax.rsqrt(variance + norm_eps) * chan_gain_in[...] + chan_shift_in[...]
+        )
+        activated = (shaped * jax.nn.sigmoid(shaped)).astype(bf16)
+        mix_out_ref[...] = jnp.dot(
+            activated, mix_out_w[...], preferred_element_type=f32
+        ).astype(bf16)
+
+    glu()
+    arrive(xin.at[rows_of(mate, cap), :], z_send.at[0], z_recv.at[0])
+    up_half(0)
+    load_down.wait()
+    down_half(0)
+    routed(1)
+    convolve()
+    load_logits.wait()
+    columns[0] = jnp.broadcast_to(place0, (128, rows)).T
+    columns[1] = jnp.broadcast_to(place1, (128, rows)).T
+    lead = logits_in[0:1, :] - logits_in[1:2, :]
+    columns[2] = jnp.broadcast_to(jax.nn.sigmoid(lead), (128, rows)).T
+    columns[3] = jnp.broadcast_to(jax.nn.sigmoid(-lead), (128, rows)).T
+    pass_on(0)
+    relay(1)
+    finish(0)
+    routed(2)
+    gathered(1)
+    up_half(1)
+    relay(2)
+    down_half(1)
+    mixer_end()
+    routed(3)
+    pass_on(1)
+    gathered(2)
+    up_half(2)
+    relay(3)
+    down_half(2)
+    finish(1)
+    pass_on(2)
+    gathered(3)
+    up_half(3)
+    down_half(3)
+    finish(2)
+    down_half(4)
+    pass_on(3)
+    acc[...] = returned(1)
+    finish(3)
+    pass_on(4)
+    arrive(ret.at[rows_of(mate, cap), :], y_send.at[0], y_recv.at[0])
+    acc[...] += returned(2) + weighted(mate * cap, cap)
+    acc[...] += returned(3)
+    finish(4)
+    out_ref[...] = (acc[...] + weighted(e * cap, cap)).astype(bf16)
+    for copy in sent:
+        copy.wait_send()
+
+
+def on_device(*args):
+    n_ep, n_tp = lax.axis_size("ep"), lax.axis_size("tp")
+    if n_tp == 4 and n_ep == 8:
+        return paired_step(*args)
+    return ring_step(*args)
+
+
+def paired_step(
+    mixer_input, mixer_gain, glu_value_weight, glu_gate_weight, conv_taps, conv_bias,
+    channel_gain, channel_shift, mixer_out_weight, expert_input, expert_gain, routes,
+    route_logits, gate_weight, up_weight, down_weight,
+):
+    n_ep, n_tp = lax.axis_size("ep"), lax.axis_size("tp")
+    rows, feat = expert_input.shape
+    cap = 3 * rows // n_ep
+    cap = -(-cap // 16) * 16
+    units = gate_weight.shape[2]
+    width = feat // n_tp
+    half = width // 2
+    n_z, pair, slots = n_ep // 2, 2 * cap, n_ep * cap
+    taken, chans, taps = mixer_input.shape[0], conv_taps.shape[0], conv_taps.shape[1]
+    keep = -(-(taps - 1) // 16) * 16
+    dma = pltpu.SemaphoreType.DMA
+    operands = (
+        expert_input, expert_gain[None, :], routes.T, route_logits.T,
+        gate_weight, up_weight, down_weight,
+        mixer_gain[None, :], conv_taps.T, conv_bias[None, :], channel_gain[None, :],
+        channel_shift[None, :], mixer_input, glu_value_weight, glu_gate_weight, mixer_out_weight,
+    )
+
+    def held(array):
+        shape = array.shape[1:] if array.ndim == 3 else array.shape
+        return pltpu.VMEM(shape, array.dtype)
+
+    block = pltpu.VMEM((n_z, pair, half), bf16)
+    blocks = pltpu.VMEM((n_z, 2, pair, half), bf16)
+    wide = pltpu.VMEM((n_z, pair, width), bf16)
+    vmem = pl.BlockSpec(memory_space=pltpu.VMEM)
+    expert_output, mixer_output = pl.pallas_call(
+        functools.partial(paired_kernel, n_ep, n_tp, cap),
+        out_shape=(
+            jax.ShapeDtypeStruct((rows, width), bf16),
+            jax.ShapeDtypeStruct((taken, mixer_out_weight.shape[1]), bf16),
+        ),
+        in_specs=[pl.BlockSpec(memory_space=pltpu.HBM)] * len(operands),
+        out_specs=(vmem, vmem),
+        scratch_shapes=[held(array) for array in operands] + [
+            pltpu.VMEM((rows, feat), bf16),
+            pltpu.VMEM((4, rows, 128), f32),
+            pltpu.VMEM((slots, width), bf16),
+            pltpu.VMEM((cap, feat), bf16),
+            pltpu.VMEM((slots, feat), bf16),
+            pltpu.VMEM((n_z, pair, units), bf16),
+            blocks, blocks, blocks, blocks, wide, block, block, block, block, block, block,
+            wide,
+            pltpu.VMEM((slots, width), bf16),
+            pltpu.VMEM((rows, width), f32),
+            dma((16 + 2 * (units // min(units, 256)),)),
+            dma((n_ep,)),
+            dma((n_ep,)),
+            dma((n_z - 1, 4)),
+            dma((n_z - 1, 4)),
+            dma((n_z + 1, 6)),
+            dma((n_z + 1, 6)),
+            dma((n_ep,)),
+            dma((n_ep,)),
+            pltpu.VMEM((taken, chans), bf16),
+            pltpu.VMEM((keep, chans), bf16),
+            pltpu.VMEM((keep + taken, chans), f32),
+            pltpu.VMEM((taken, chans), bf16),
+            pltpu.VMEM((n_tp, taken, chans), bf16),
+            dma((2,)),
+            dma((n_tp - 1,)),
+            dma((n_tp - 1,)),
+        ],
+        compiler_params=pltpu.CompilerParams(
+            collective_id=0, has_side_effects=True, vmem_limit_bytes=56 * 1024 * 1024
+        ),
+        cost_estimate=pl.CostEstimate(
+            flops=6 * slots * feat * units, bytes_accessed=6 * feat * units, transcendentals=0
+        ),
+    )(*operands)
+    return (mixer_output, expert_output)
+
+
+def ring_step(
     mixer_input, mixer_gain, glu_value_weight, glu_gate_weight, conv_taps, conv_bias,
     channel_gain, channel_shift, mixer_out_weight, expert_input, expert_gain, routes,
     route_logits, gate_weight, up_weight, down_weight,

time: 100 us -> 75.1 us (0.75)
  Pallas kernels: 85.5 us -> 71.1 us
  local copies, waits for them, and re-layouts: 13.2 us -> 3.24 us
    pallas_call x1, Pallas kernels: 85.5 us -> 71.1 us  [paired_step(): pl.pallas_call(functools.partial(paired_kernel, n_ep, n_tp, cap), out_sha...]
    unnamed x28 -> x2, local copies, waits for them, and re-layouts: 13.2 us -> 3.24 us
where the time goes in v1:
time: 75.1 us; the launch traced here: 75 us
  Pallas kernels  71.1 us (95%)
  local copies, waits for them, and re-layouts  3.24 us (4%)
    pallas_call x1, Pallas kernels, paired_step(): pl.pallas_call(functools.partial(paired_kernel, n_ep, n_tp, cap), out_sha...  71.1 us
    unnamed x2, local copies, waits for them, and re-layouts  3.24 us

profile of v1, /device:TPU:1, one launch (start us, length us, event | category | flops | bytes accessed | tf_op | source)
XLA Modules:
  0.0 75.0 jit_solution(3849444390838250769)
XLA Ops:
  0.6 71.1 %shard_map.167 = (bf16[256,512]{1,0:T(8,128)(2,1)}, bf16[128,512]{1,0:T(8,128)(2,1)}) custom-call(bf16[256,2048]{1,0:T(8,128)(2,1)} %x_hbm.1, f32[1,2048]{1,0:T(1,128)} %bitcast.9, s32[2,256]{1,0:T(2,128)} %bitcast.11, f32[2,256]{1,0:T(2,128)} %bitcast.12, bf16[1,2048,1024]{2,1,0:T(8,128)(2,1)} %gate_hbm.1, bf16[1,2048,1024]{2,1,0:T(8,128)(2,1)} %up_hbm.1, ...), custom_call_target="tpu_custom_call" | custom-call | flops 9663676416 | bytes 12582912 | tf_op jit(solution)/shard_map/pallas_call | solution.py:775
  71.7 1.6 %copy.20 = bf16[128,512]{1,0:T(8,128)(2,1)} copy(bf16[128,512]{1,0:T(8,128)(2,1)} %get-tuple-element.8) | data formatting | bytes 262144
  73.3 1.7 %copy.21 = bf16[256,512]{1,0:T(8,128)(2,1)} copy(bf16[256,512]{1,0:T(8,128)(2,1)} %get-tuple-element.9) | data formatting | bytes 524288

commit v2 on v1

--- a/solution.py
+++ b/solution.py
@@ -345,6 +345,20 @@
         copy.wait_send()
 
 
+outer_plan = (
+    "pass0", "route2", "relay2", "route3", "join2", "up2", "more2", "far2", "relay3", "conv",
+    "route1", "near2", "own2", "pass2", "up1", "more1", "far1", "join3", "up3", "more3", "far3",
+    "spread", "sum2", "sum0", "near3", "pass3", "near1", "own3", "mix", "back0", "sum3", "pass1",
+    "own1", "sum1", "back2", "back3", "back1",
+)
+inner_plan = (
+    "pass0", "route2", "relay2", "route3", "join2", "up2", "more2", "far2", "relay3", "conv",
+    "near2", "pass2", "join3", "up3", "more3", "far3", "own2", "near3", "sum2", "route1", "spread",
+    "up1", "pass3", "more1", "far1", "own3", "near1", "mix", "pass1", "sum0", "back2", "back0",
+    "own1", "sum3", "sum1", "back3", "back1",
+)
+
+
 def paired_kernel(
     n_ep, n_tp, cap,
     x_hbm, gain_hbm, routes_hbm, logits_hbm, gate_hbm, up_hbm, down_hbm,
@@ -354,7 +368,7 @@
     x_in, gain_in, routes_in, logits_in, gate_w, up_w, down_w,
     mix_gain_in, taps_in, bias_in, chan_gain_in, chan_shift_in,
     mix_in, value_w, glu_gate_w, mix_out_w,
-    normed, columns, out_part, out_pair, xin, hidden,
+    normed, columns, out_part, out_pair, out_near, xin, hidden,
     part_x, part_y, got_x, got_y, held_own, held_x, held_y, pass_x, pass_y, last_x, last_y,
     summed, ret, acc,
     load_sem, z_send, z_recv, ag_send, ag_recv, rs_send, rs_recv, y_send, y_recv,
@@ -368,7 +382,7 @@
     c = e % 2
     mate = e + 1 - 2 * c
     rows, feat = x_in.shape
-    width = out_part.shape[1]
+    width = out_part.shape[2]
     half = width // 2
     pair = 2 * cap
     slots = n_ep * cap
@@ -381,6 +395,8 @@
 
     def chip_of(k):
         return [z, z + 1 - 2 * (z % 2), (z + 2) % 4, 3 - z][k]
+
+    inner = (z + 1) // 2 % 2
 
     def rows_of(index, count):
         return pl.ds(pl.multiple_of(index * count, count), count)
@@ -449,9 +465,11 @@
     values = x_in[...].astype(f32)
     scale = lax.rsqrt(jnp.mean(values * values, axis=-1, keepdims=True) + norm_eps)
     normed[...] = (values * scale * gain_in[...]).astype(bf16)
-    out_part[...] = jnp.dot(
-        pick(0, slots), normed[:, cols(t, 0, width)], preferred_element_type=f32
-    ).astype(bf16)
+    for k in (2, 3):
+        out_part[k - 2] = jnp.dot(
+            pick(chip_of(k) * pair, pair), normed[:, cols(t, 0, width)],
+            preferred_element_type=f32,
+        ).astype(bf16)
 
     pl.semaphore_wait(barrier, n_ep - 1 + n_tp - 1)
 
@@ -471,11 +489,12 @@
             device_id=(mate, t), device_id_type=MESH,
         ).wait_recv()
 
-    for k in range(1, n_z):
+    for k in (2, 3):
         for cc in range(2):
             dest = chip_of(k) * 2 + cc
             send(
-                out_part.at[rows_of(dest, cap), :], xin.at[rows_of(e, cap), cols(t, 0, width)],
+                out_part.at[k - 2, pl.ds(cc * cap, cap), :],
+                xin.at[rows_of(e, cap), cols(t, 0, width)],
                 z_send.at[2 * k + cc], z_recv.at[2 * k + c], (dest, t),
             )
 
@@ -483,35 +502,47 @@
         pick(mate * cap, cap), normed[...], preferred_element_type=f32
     ).astype(bf16)
     send(out_pair, xin.at[rows_of(e, cap), :], z_send.at[0], z_recv.at[0], (mate, t))
+    for cc in range(2):
+        dest = chip_of(1) * 2 + cc
+        out_near[cc] = jnp.dot(
+            pick(dest * cap, cap), normed[...], preferred_element_type=f32
+        ).astype(bf16)
+        send(
+            out_near.at[cc], xin.at[rows_of(e, cap), :],
+            z_send.at[2 + cc], z_recv.at[2 + c], (dest, t),
+        )
     xin[rows_of(e, cap), :] = jnp.dot(
         pick(e * cap, cap), normed[...], preferred_element_type=f32
     ).astype(bf16)
 
     def routed(k):
         for cc in range(2):
+            here = rows_of(chip_of(k) * 2 + cc, cap)
             arrive(
-                xin.at[rows_of(chip_of(k) * 2 + cc, cap), cols(t, 0, width)],
+                xin.at[here, :] if k == 1 else xin.at[here, cols(t, 0, width)],
                 z_send.at[2 * k + cc], z_recv.at[2 * k + cc],
             )
+        if k == 1:
+            return
         block = xin.at[rows_of(chip_of(k), pair), cols(t, 0, width)]
-        send(block, block, ag_send.at[k - 1, 0], ag_recv.at[k - 1, 0], (e, t_x))
-        send(block, block, ag_send.at[k - 1, 1], ag_recv.at[k - 1, 1], (e, t_y))
+        send(block, block, ag_send.at[k - 2, 0], ag_recv.at[k - 2, 0], (e, t_x))
+        send(block, block, ag_send.at[k - 2, 1], ag_recv.at[k - 2, 1], (e, t_y))
 
     def relay(k):
         here = rows_of(chip_of(k), pair)
-        arrive(xin.at[here, cols(t_y, 0, width)], ag_send.at[k - 1, 1], ag_recv.at[k - 1, 1])
+        arrive(xin.at[here, cols(t_y, 0, width)], ag_send.at[k - 2, 1], ag_recv.at[k - 2, 1])
         block = xin.at[here, cols(t_y, 0, half)]
-        send(block, block, ag_send.at[k - 1, 2], ag_recv.at[k - 1, 2], (e, t_x))
-        arrive(xin.at[here, cols(t_x, 0, width)], ag_send.at[k - 1, 0], ag_recv.at[k - 1, 0])
+        send(block, block, ag_send.at[k - 2, 2], ag_recv.at[k - 2, 2], (e, t_x))
+        arrive(xin.at[here, cols(t_x, 0, width)], ag_send.at[k - 2, 0], ag_recv.at[k - 2, 0])
         block = xin.at[here, cols(t_x, half, half)]
-        send(block, block, ag_send.at[k - 1, 3], ag_recv.at[k - 1, 3], (e, t_y))
+        send(block, block, ag_send.at[k - 2, 3], ag_recv.at[k - 2, 3], (e, t_y))
 
     def gathered(k):
         here = rows_of(chip_of(k), pair)
-        arrive(xin.at[here, cols(t_d, 0, half)], ag_send.at[k - 1, 2], ag_recv.at[k - 1, 2])
-        arrive(xin.at[here, cols(t_d, half, half)], ag_send.at[k - 1, 3], ag_recv.at[k - 1, 3])
-
-    def up_half(k):
+        arrive(xin.at[here, cols(t_d, 0, half)], ag_send.at[k - 2, 2], ag_recv.at[k - 2, 2])
+        arrive(xin.at[here, cols(t_d, half, half)], ag_send.at[k - 2, 3], ag_recv.at[k - 2, 3])
+
+    def up_half(k, first, last):
         here = rows_of(chip_of(k), pair)
 
         def one(j, carry):
@@ -525,84 +556,63 @@
             hidden[k, :, at] = (g * jax.nn.sigmoid(g) * u).astype(bf16)
             return carry
 
-        lax.fori_loop(0, tiles, one, 0)
-
-    def group(u):
-        if u == 0:
-            return 0, rows_of(1 - c, cap), pl.ds(0, cap)
-        if u == n_z:
-            return 0, rows_of(c, cap), pl.ds(cap, cap)
-        return u, pl.ds(0, pair), pl.ds(0, pair)
-
-    def down_half(u):
-        k, here, at = group(u)
-
-        def product(quarter):
-            return jnp.dot(
-                hidden[k, here, :], down_w[:, cols(quarter, 0, width)],
-                preferred_element_type=f32,
-            ).astype(bf16)
-
-        def give(src, dst, way, to):
-            send(src, dst, rs_send.at[u, way], rs_recv.at[u, way], (e, to))
-
-        far = product(t_d)
-        part_x[k, 1, at, :] = far[:, :half]
-        part_y[k, 1, at, :] = far[:, half:]
-        give(part_x.at[k, 1, at, :], got_x.at[k, 1, at, :], 0, t_x)
-        give(part_y.at[k, 1, at, :], got_y.at[k, 1, at, :], 1, t_y)
-        near = product(t_x)
-        part_x[k, 0, at, :] = near[:, :half]
-        held_x[k, at, :] = near[:, half:]
-        give(part_x.at[k, 0, at, :], got_x.at[k, 0, at, :], 2, t_x)
-        near = product(t_y)
-        part_y[k, 0, at, :] = near[:, half:]
-        held_y[k, at, :] = near[:, :half]
-        give(part_y.at[k, 0, at, :], got_y.at[k, 0, at, :], 3, t_y)
-        held_own[k, at, :] = product(t)
-
-    def pass_on(u):
-        k, here, at = group(u)
-        arrive(got_x.at[k, 1, at, :], rs_send.at[u, 0], rs_recv.at[u, 0])
-        pass_y[k, at, :] = (
-            held_y[k, at, :].astype(f32) + got_x[k, 1, at, :].astype(f32)
+        lax.fori_loop(first, last, one, 0)
+
+    def product(k, quarter):
+        return jnp.dot(
+            hidden[k], down_w[:, cols(quarter, 0, width)], preferred_element_type=f32
         ).astype(bf16)
-        send(
-            pass_y.at[k, at, :], last_y.at[k, at, :], rs_send.at[u, 4], rs_recv.at[u, 4], (e, t_y)
-        )
-        arrive(got_y.at[k, 1, at, :], rs_send.at[u, 1], rs_recv.at[u, 1])
-        pass_x[k, at, :] = (
-            held_x[k, at, :].astype(f32) + got_y[k, 1, at, :].astype(f32)
+
+    def give(k, way, src, dst, to):
+        send(src, dst, rs_send.at[k, way], rs_recv.at[k, way], (e, to))
+
+    def down_far(k):
+        far = product(k, t_d)
+        part_x[k, 1] = far[:, :half]
+        part_y[k, 1] = far[:, half:]
+        give(k, 0, part_x.at[k, 1], got_x.at[k, 1], t_x)
+        give(k, 1, part_y.at[k, 1], got_y.at[k, 1], t_y)
+
+    def down_near(k):
+        near = product(k, t_x)
+        part_x[k, 0] = near[:, :half]
+        held_x[k] = near[:, half:]
+        give(k, 2, part_x.at[k, 0], got_x.at[k, 0], t_x)
+        near = product(k, t_y)
+        part_y[k, 0] = near[:, half:]
+        held_y[k] = near[:, :half]
+        give(k, 3, part_y.at[k, 0], got_y.at[k, 0], t_y)
+
+    def down_own(k):
+        held_own[k] = product(k, t)
+
+    def pass_on(k):
+        arrive(got_x.at[k, 1], rs_send.at[k, 0], rs_recv.at[k, 0])
+        pass_y[k] = (held_y[k].astype(f32) + got_x[k, 1].astype(f32)).astype(bf16)
+        give(k, 4, pass_y.at[k], last_y.at[k], t_y)
+        arrive(got_y.at[k, 1], rs_send.at[k, 1], rs_recv.at[k, 1])
+        pass_x[k] = (held_x[k].astype(f32) + got_y[k, 1].astype(f32)).astype(bf16)
+        give(k, 5, pass_x.at[k], last_x.at[k], t_x)
+
+    def finish(k):
+        arrive(got_x.at[k, 0], rs_send.at[k, 2], rs_recv.at[k, 2])
+        arrive(got_y.at[k, 0], rs_send.at[k, 3], rs_recv.at[k, 3])
+        arrive(last_y.at[k], rs_send.at[k, 4], rs_recv.at[k, 4])
+        arrive(last_x.at[k], rs_send.at[k, 5], rs_recv.at[k, 5])
+        summed[k, :, :half] = (
+            held_own[k, :, :half].astype(f32)
+            + got_x[k, 0].astype(f32) + last_y[k].astype(f32)
         ).astype(bf16)
-        send(
-            pass_x.at[k, at, :], last_x.at[k, at, :], rs_send.at[u, 5], rs_recv.at[u, 5], (e, t_x)
-        )
-
-    def finish(u):
-        k, here, at = group(u)
-        arrive(got_x.at[k, 0, at, :], rs_send.at[u, 2], rs_recv.at[u, 2])
-        arrive(got_y.at[k, 0, at, :], rs_send.at[u, 3], rs_recv.at[u, 3])
-        arrive(last_y.at[k, at, :], rs_send.at[u, 4], rs_recv.at[u, 4])
-        arrive(last_x.at[k, at, :], rs_send.at[u, 5], rs_recv.at[u, 5])
-        low = (
-            held_own[k, at, :half].astype(f32)
-            + got_x[k, 0, at, :].astype(f32) + last_y[k, at, :].astype(f32)
+        summed[k, :, half:] = (
+            held_own[k, :, half:].astype(f32)
+            + got_y[k, 0].astype(f32) + last_x[k].astype(f32)
         ).astype(bf16)
-        high = (
-            held_own[k, at, half:].astype(f32)
-            + got_y[k, 0, at, :].astype(f32) + last_x[k, at, :].astype(f32)
-        ).astype(bf16)
-        if u == n_z:
-            ret[rows_of(e, cap), :half] = low
-            ret[rows_of(e, cap), half:] = high
-            return
-        summed[k, at, :half] = low
-        summed[k, at, half:] = high
-        if u == 0:
+        if k == 0:
             send(
-                summed.at[0, pl.ds(0, cap), :], ret.at[rows_of(e, cap), :],
+                summed.at[0, rows_of(1 - c, cap), :], ret.at[rows_of(e, cap), :],
                 y_send.at[0], y_recv.at[0], (mate, t),
             )
+            ret[rows_of(e, cap), :] = summed[0, rows_of(c, cap), :]
             return
         for cc in range(2):
             send(
@@ -624,7 +634,9 @@
         return one * columns[2, :, 0:1] + two * columns[3, :, 0:1]
 
     def returned(k):
-        for cc in range(2):
+        if k == 0:
+            arrive(ret.at[rows_of(mate, cap), :], y_send.at[0], y_recv.at[0])
+        for cc in range(2 if k > 0 else 0):
             arrive(
                 ret.at[rows_of(chip_of(k) * 2 + cc, cap), :],
                 y_send.at[2 * k + cc], y_recv.at[2 * k + cc],
@@ -686,50 +698,55 @@
             activated, mix_out_w[...], preferred_element_type=f32
         ).astype(bf16)
 
+    def spread():
+        load_logits.wait()
+        columns[0] = jnp.broadcast_to(place0, (128, rows)).T
+        columns[1] = jnp.broadcast_to(place1, (128, rows)).T
+        lead = logits_in[0:1, :] - logits_in[1:2, :]
+        columns[2] = jnp.broadcast_to(jax.nn.sigmoid(lead), (128, rows)).T
+        columns[3] = jnp.broadcast_to(jax.nn.sigmoid(-lead), (128, rows)).T
+
+    steps = {
+        "route": routed, "relay": relay, "join": gathered,
+        "up": lambda k: up_half(k, 0, tiles // 2), "more": lambda k: up_half(k, tiles // 2, tiles),
+        "far": down_far, "near": down_near, "own": down_own,
+        "pass": pass_on, "sum": finish, "spread": spread, "conv": convolve, "mix": mixer_end,
+    }
+
+    def run(plan):
+        back = []
+        for step in plan:
+            name, at = step.rstrip("0123"), [int(step[-1])] if step[-1].isdigit() else []
+            with jax.named_scope(step):
+                if name != "back":
+                    steps[name](*at)
+                    continue
+                part = returned(*at)
+                back.append(step)
+                if len(back) == 1:
+                    acc[...] = part
+                elif len(back) < n_z:
+                    acc[...] += part
+                else:
+                    out_ref[...] = (acc[...] + part).astype(bf16)
+
     glu()
     arrive(xin.at[rows_of(mate, cap), :], z_send.at[0], z_recv.at[0])
-    up_half(0)
+    up_half(0, 0, tiles)
     load_down.wait()
-    down_half(0)
-    routed(1)
-    convolve()
-    load_logits.wait()
-    columns[0] = jnp.broadcast_to(place0, (128, rows)).T
-    columns[1] = jnp.broadcast_to(place1, (128, rows)).T
-    lead = logits_in[0:1, :] - logits_in[1:2, :]
-    columns[2] = jnp.broadcast_to(jax.nn.sigmoid(lead), (128, rows)).T
-    columns[3] = jnp.broadcast_to(jax.nn.sigmoid(-lead), (128, rows)).T
-    pass_on(0)
-    relay(1)
-    finish(0)
-    routed(2)
-    gathered(1)
-    up_half(1)
-    relay(2)
-    down_half(1)
-    mixer_end()
-    routed(3)
-    pass_on(1)
-    gathered(2)
-    up_half(2)
-    relay(3)
-    down_half(2)
-    finish(1)
-    pass_on(2)
-    gathered(3)
-    up_half(3)
-    down_half(3)
-    finish(2)
-    down_half(4)
-    pass_on(3)
-    acc[...] = returned(1)
-    finish(3)
-    pass_on(4)
-    arrive(ret.at[rows_of(mate, cap), :], y_send.at[0], y_recv.at[0])
-    acc[...] += returned(2) + weighted(mate * cap, cap)
-    acc[...] += returned(3)
-    finish(4)
-    out_ref[...] = (acc[...] + weighted(e * cap, cap)).astype(bf16)
+    down_far(0)
+    down_near(0)
+    down_own(0)
+    early = len(sent)
+    for side, plan in ((0, outer_plan), (1, inner_plan)):
+
+        @pl.when(inner == side)
+        def one_side(plan=plan):
+            run(plan)
+            for copy in sent[early:]:
+                copy.wait_send()
+            del sent[early:]
+
     for copy in sent:
         copy.wait_send()
 
@@ -783,8 +800,9 @@
         scratch_shapes=[held(array) for array in operands] + [
             pltpu.VMEM((rows, feat), bf16),
             pltpu.VMEM((4, rows, 128), f32),
-            pltpu.VMEM((slots, width), bf16),
+            pltpu.VMEM((2, pair, width), bf16),
             pltpu.VMEM((cap, feat), bf16),
+            pltpu.VMEM((2, cap, feat), bf16),
             pltpu.VMEM((slots, feat), bf16),
             pltpu.VMEM((n_z, pair, units), bf16),
             blocks, blocks, blocks, blocks, wide, block, block, block, block, block, block,
@@ -794,10 +812,10 @@
             dma((16 + 2 * (units // min(units, 256)),)),
             dma((n_ep,)),
             dma((n_ep,)),
-            dma((n_z - 1, 4)),
-            dma((n_z - 1, 4)),
-            dma((n_z + 1, 6)),
-            dma((n_z + 1, 6)),
+            dma((n_z - 2, 4)),
+            dma((n_z - 2, 4)),
+            dma((n_z, 6)),
+            dma((n_z, 6)),
             dma((n_ep,)),
             dma((n_ep,)),
             pltpu.VMEM((taken, chans), bf16),

time: 75.1 us -> 69.8 us (0.929)
  Pallas kernels: 71.1 us -> 65.8 us
    pallas_call x1, Pallas kernels: 71.1 us -> 65.8 us  [paired_step(): pl.pallas_call(functools.partial(paired_kernel, n_ep, n_tp, cap), out_sha...]
where the time goes in v2:
time: 69.8 us; the launch traced here: 69.7 us
  Pallas kernels  65.8 us (94%)
  local copies, waits for them, and re-layouts  3.24 us (5%)
    pallas_call x1, Pallas kernels, paired_step(): pl.pallas_call(functools.partial(paired_kernel, n_ep, n_tp, cap), out_sha...  65.8 us
    unnamed x2, local copies, waits for them, and re-layouts  3.24 us

profile of v2, /device:TPU:1, one launch (start us, length us, event | category | flops | bytes accessed | tf_op | source)
XLA Modules:
  0.0 69.7 jit_solution(8925179451961765952)
XLA Ops:
  0.6 65.8 %shard_map.167 = (bf16[256,512]{1,0:T(8,128)(2,1)}, bf16[128,512]{1,0:T(8,128)(2,1)}) custom-call(bf16[256,2048]{1,0:T(8,128)(2,1)} %x_hbm.1, f32[1,2048]{1,0:T(1,128)} %bitcast.9, s32[2,256]{1,0:T(2,128)} %bitcast.11, f32[2,256]{1,0:T(2,128)} %bitcast.12, bf16[1,2048,1024]{2,1,0:T(8,128)(2,1)} %gate_hbm.1, bf16[1,2048,1024]{2,1,0:T(8,128)(2,1)} %up_hbm.1, ...), custom_call_target="tpu_custom_call" | custom-call | flops 9663676416 | bytes 12582912 | tf_op jit(solution)/shard_map/pallas_call | solution.py:792
  66.4 1.6 %copy.20 = bf16[128,512]{1,0:T(8,128)(2,1)} copy(bf16[128,512]{1,0:T(8,128)(2,1)} %get-tuple-element.8) | data formatting | bytes 262144
  68.0 1.7 %copy.21 = bf16[256,512]{1,0:T(8,128)(2,1)} copy(bf16[256,512]{1,0:T(8,128)(2,1)} %get-tuple-element.9) | data formatting | bytes 524288

commit v3 on v2

--- a/solution.py
+++ b/solution.py
@@ -346,16 +346,24 @@
 
 
 outer_plan = (
-    "pass0", "route2", "relay2", "route3", "join2", "up2", "more2", "far2", "relay3", "conv",
-    "route1", "near2", "own2", "pass2", "up1", "more1", "far1", "join3", "up3", "more3", "far3",
-    "spread", "sum2", "sum0", "near3", "pass3", "near1", "own3", "mix", "back0", "sum3", "pass1",
-    "own1", "sum1", "back2", "back3", "back1",
+    "far00", "near00", "route20", "pass00", "route21", "relay20", "own00", "pass01", "relay21",
+    "route30", "join20", "spread", "up20", "more20", "far20", "route10", "up10", "join21",
+    "route31", "relay30", "sum01", "near20", "up21", "more21", "more10", "relay31", "far21",
+    "near21", "join30", "up30", "more30", "far30", "pass20", "join31", "up31", "conv", "more31",
+    "pass21", "near30", "own20", "pass30", "own21", "far31", "route11", "own30", "near31", "sum20",
+    "sum21", "own31", "up11", "far10", "sum00", "more11", "sum30", "pass31", "near10", "far11",
+    "own10", "pass10", "near11", "sum31", "pass11", "back2", "sum10", "back01", "own11", "sum11",
+    "mix", "back3", "back00", "back1",
 )
 inner_plan = (
-    "pass0", "route2", "relay2", "route3", "join2", "up2", "more2", "far2", "relay3", "conv",
-    "near2", "pass2", "join3", "up3", "more3", "far3", "own2", "near3", "sum2", "route1", "spread",
-    "up1", "pass3", "more1", "far1", "own3", "near1", "mix", "pass1", "sum0", "back2", "back0",
-    "own1", "sum3", "sum1", "back3", "back1",
+    "far00", "route20", "pass01", "near00", "relay20", "route21", "route30", "relay21", "pass00",
+    "join20", "up20", "more20", "far20", "join21", "relay30", "up21", "route31", "own00", "more21",
+    "far21", "near20", "join30", "pass20", "own20", "up30", "near21", "more30", "sum01", "spread",
+    "sum00", "own21", "conv", "pass21", "back00", "route10", "relay31", "up10", "sum20", "more10",
+    "far10", "far30", "sum21", "near30", "near10", "own30", "pass10", "join31", "up31", "own10",
+    "pass30", "more31", "far31", "near31", "route11", "up11", "more11", "far11", "own31", "near11",
+    "pass31", "pass11", "own11", "sum10", "sum30", "back01", "back2", "sum31", "sum11", "mix",
+    "back3", "back1",
 )
 
 
@@ -368,7 +376,7 @@
     x_in, gain_in, routes_in, logits_in, gate_w, up_w, down_w,
     mix_gain_in, taps_in, bias_in, chan_gain_in, chan_shift_in,
     mix_in, value_w, glu_gate_w, mix_out_w,
-    normed, columns, out_part, out_pair, out_near, xin, hidden,
+    normed, columns, out_part, out_pair, out_near, xin, hidden_own, hidden,
     part_x, part_y, got_x, got_y, held_own, held_x, held_y, pass_x, pass_y, last_x, last_y,
     summed, ret, acc,
     load_sem, z_send, z_recv, ag_send, ag_recv, rs_send, rs_recv, y_send, y_recv,
@@ -382,7 +390,7 @@
     c = e % 2
     mate = e + 1 - 2 * c
     rows, feat = x_in.shape
-    width = out_part.shape[2]
+    width = ret.shape[1]
     half = width // 2
     pair = 2 * cap
     slots = n_ep * cap
@@ -489,136 +497,144 @@
             device_id=(mate, t), device_id_type=MESH,
         ).wait_recv()
 
+    def core_of(h):
+        return 1 - c if h else c
+
+    def peer(k, h):
+        return chip_of(k) * 2 + core_of(h)
+
     for k in (2, 3):
-        for cc in range(2):
-            dest = chip_of(k) * 2 + cc
+        for h in range(2):
             send(
-                out_part.at[k - 2, pl.ds(cc * cap, cap), :],
+                out_part.at[k - 2, rows_of(core_of(h), cap), :],
                 xin.at[rows_of(e, cap), cols(t, 0, width)],
-                z_send.at[2 * k + cc], z_recv.at[2 * k + c], (dest, t),
+                z_send.at[k, h], z_recv.at[k, h], (peer(k, h), t),
             )
 
     out_pair[...] = jnp.dot(
         pick(mate * cap, cap), normed[...], preferred_element_type=f32
     ).astype(bf16)
-    send(out_pair, xin.at[rows_of(e, cap), :], z_send.at[0], z_recv.at[0], (mate, t))
-    for cc in range(2):
-        dest = chip_of(1) * 2 + cc
-        out_near[cc] = jnp.dot(
-            pick(dest * cap, cap), normed[...], preferred_element_type=f32
+    send(out_pair, xin.at[rows_of(e, cap), :], z_send.at[0, 1], z_recv.at[0, 1], (mate, t))
+    for h in range(2):
+        out_near[h] = jnp.dot(
+            pick(peer(1, h) * cap, cap), normed[...], preferred_element_type=f32
         ).astype(bf16)
         send(
-            out_near.at[cc], xin.at[rows_of(e, cap), :],
-            z_send.at[2 + cc], z_recv.at[2 + c], (dest, t),
+            out_near.at[h], xin.at[rows_of(e, cap), :],
+            z_send.at[1, h], z_recv.at[1, h], (peer(1, h), t),
         )
     xin[rows_of(e, cap), :] = jnp.dot(
         pick(e * cap, cap), normed[...], preferred_element_type=f32
     ).astype(bf16)
 
-    def routed(k):
-        for cc in range(2):
-            here = rows_of(chip_of(k) * 2 + cc, cap)
-            arrive(
-                xin.at[here, :] if k == 1 else xin.at[here, cols(t, 0, width)],
-                z_send.at[2 * k + cc], z_recv.at[2 * k + cc],
-            )
-        if k == 1:
+    def route(k, h):
+        here = rows_of(peer(k, h), cap)
+        block = xin.at[here, :] if k == 1 else xin.at[here, cols(t, 0, width)]
+        arrive(block, z_send.at[k, h], z_recv.at[k, h])
+        if k > 1:
+            send(block, block, ag_send.at[k - 2, h, 0], ag_recv.at[k - 2, h, 0], (e, t_x))
+            send(block, block, ag_send.at[k - 2, h, 1], ag_recv.at[k - 2, h, 1], (e, t_y))
+
+    def relay(k, h):
+        here = rows_of(peer(k, h), cap)
+        sends, recvs = ag_send.at[k - 2, h], ag_recv.at[k - 2, h]
+        arrive(xin.at[here, cols(t_y, 0, width)], sends.at[1], recvs.at[1])
+        block = xin.at[here, cols(t_y, 0, half)]
+        send(block, block, sends.at[2], recvs.at[2], (e, t_x))
+        arrive(xin.at[here, cols(t_x, 0, width)], sends.at[0], recvs.at[0])
+        block = xin.at[here, cols(t_x, half, half)]
+        send(block, block, sends.at[3], recvs.at[3], (e, t_y))
+
+    def join(k, h):
+        here = rows_of(peer(k, h), cap)
+        sends, recvs = ag_send.at[k - 2, h], ag_recv.at[k - 2, h]
+        arrive(xin.at[here, cols(t_d, 0, half)], sends.at[2], recvs.at[2])
+        arrive(xin.at[here, cols(t_d, half, half)], sends.at[3], recvs.at[3])
+
+    def gated_units(rows_in, j):
+        at = pl.ds(pl.multiple_of(j * tile, tile), tile)
+        g = jnp.dot(rows_in, gate_w[:, at], preferred_element_type=f32)
+        u = jnp.dot(rows_in, up_w[:, at], preferred_element_type=f32)
+        return at, (g * jax.nn.sigmoid(g) * u).astype(bf16)
+
+    def up_own():
+        def one(j, carry):
+            for copy in weight_tile(j):
+                copy.wait()
+            at, block = gated_units(xin[rows_of(z, pair), :], j)
+            hidden_own[:, at] = block
+            return carry
+
+        lax.fori_loop(0, tiles, one, 0)
+
+    def up_part(k, h, first, last):
+        def one(j, carry):
+            at, block = gated_units(xin[rows_of(peer(k, h), cap), :], j)
+            hidden[k - 1, h, :, at] = block
+            return carry
+
+        lax.fori_loop(first, last, one, 0)
+
+    def product(k, h, quarter):
+        block = hidden[k - 1, h] if k else hidden_own[rows_of(core_of(h), cap), :]
+        return jnp.dot(
+            block, down_w[:, cols(quarter, 0, width)], preferred_element_type=f32
+        ).astype(bf16)
+
+    def give(k, h, way, src, dst, to):
+        send(src, dst, rs_send.at[k, h, way], rs_recv.at[k, h, way], (e, to))
+
+    def down_far(k, h):
+        far = product(k, h, t_d)
+        part_x[k, h, 1] = far[:, :half]
+        part_y[k, h, 1] = far[:, half:]
+        give(k, h, 0, part_x.at[k, h, 1], got_x.at[k, h, 1], t_x)
+        give(k, h, 1, part_y.at[k, h, 1], got_y.at[k, h, 1], t_y)
+
+    def down_near(k, h):
+        near = product(k, h, t_x)
+        part_x[k, h, 0] = near[:, :half]
+        held_x[k, h] = near[:, half:]
+        give(k, h, 2, part_x.at[k, h, 0], got_x.at[k, h, 0], t_x)
+        near = product(k, h, t_y)
+        part_y[k, h, 0] = near[:, half:]
+        held_y[k, h] = near[:, :half]
+        give(k, h, 3, part_y.at[k, h, 0], got_y.at[k, h, 0], t_y)
+
+    def down_own(k, h):
+        held_own[k, h] = product(k, h, t)
+
+    def pass_on(k, h):
+        arrive(got_x.at[k, h, 1], rs_send.at[k, h, 0], rs_recv.at[k, h, 0])
+        pass_y[k, h] = (held_y[k, h].astype(f32) + got_x[k, h, 1].astype(f32)).astype(bf16)
+        give(k, h, 4, pass_y.at[k, h], last_y.at[k, h], t_y)
+        arrive(got_y.at[k, h, 1], rs_send.at[k, h, 1], rs_recv.at[k, h, 1])
+        pass_x[k, h] = (held_x[k, h].astype(f32) + got_y[k, h, 1].astype(f32)).astype(bf16)
+        give(k, h, 5, pass_x.at[k, h], last_x.at[k, h], t_x)
+
+    def finish(k, h):
+        arrive(got_x.at[k, h, 0], rs_send.at[k, h, 2], rs_recv.at[k, h, 2])
+        arrive(got_y.at[k, h, 0], rs_send.at[k, h, 3], rs_recv.at[k, h, 3])
+        arrive(last_y.at[k, h], rs_send.at[k, h, 4], rs_recv.at[k, h, 4])
+        arrive(last_x.at[k, h], rs_send.at[k, h, 5], rs_recv.at[k, h, 5])
+        low = (
+            held_own[k, h, :, :half].astype(f32)
+            + got_x[k, h, 0].astype(f32) + last_y[k, h].astype(f32)
+        ).astype(bf16)
+        high = (
+            held_own[k, h, :, half:].astype(f32)
+            + got_y[k, h, 0].astype(f32) + last_x[k, h].astype(f32)
+        ).astype(bf16)
+        if k == 0 and h == 0:
+            ret[rows_of(e, cap), :half] = low
+            ret[rows_of(e, cap), half:] = high
             return
-        block = xin.at[rows_of(chip_of(k), pair), cols(t, 0, width)]
-        send(block, block, ag_send.at[k - 2, 0], ag_recv.at[k - 2, 0], (e, t_x))
-        send(block, block, ag_send.at[k - 2, 1], ag_recv.at[k - 2, 1], (e, t_y))
-
-    def relay(k):
-        here = rows_of(chip_of(k), pair)
-        arrive(xin.at[here, cols(t_y, 0, width)], ag_send.at[k - 2, 1], ag_recv.at[k - 2, 1])
-        block = xin.at[here, cols(t_y, 0, half)]
-        send(block, block, ag_send.at[k - 2, 2], ag_recv.at[k - 2, 2], (e, t_x))
-        arrive(xin.at[here, cols(t_x, 0, width)], ag_send.at[k - 2, 0], ag_recv.at[k - 2, 0])
-        block = xin.at[here, cols(t_x, half, half)]
-        send(block, block, ag_send.at[k - 2, 3], ag_recv.at[k - 2, 3], (e, t_y))
-
-    def gathered(k):
-        here = rows_of(chip_of(k), pair)
-        arrive(xin.at[here, cols(t_d, 0, half)], ag_send.at[k - 2, 2], ag_recv.at[k - 2, 2])
-        arrive(xin.at[here, cols(t_d, half, half)], ag_send.at[k - 2, 3], ag_recv.at[k - 2, 3])
-
-    def up_half(k, first, last):
-        here = rows_of(chip_of(k), pair)
-
-        def one(j, carry):
-            if k == 0:
-                for copy in weight_tile(j):
-                    copy.wait()
-            at = pl.ds(pl.multiple_of(j * tile, tile), tile)
-            rows_in = xin[here, :]
-            g = jnp.dot(rows_in, gate_w[:, at], preferred_element_type=f32)
-            u = jnp.dot(rows_in, up_w[:, at], preferred_element_type=f32)
-            hidden[k, :, at] = (g * jax.nn.sigmoid(g) * u).astype(bf16)
-            return carry
-
-        lax.fori_loop(first, last, one, 0)
-
-    def product(k, quarter):
-        return jnp.dot(
-            hidden[k], down_w[:, cols(quarter, 0, width)], preferred_element_type=f32
-        ).astype(bf16)
-
-    def give(k, way, src, dst, to):
-        send(src, dst, rs_send.at[k, way], rs_recv.at[k, way], (e, to))
-
-    def down_far(k):
-        far = product(k, t_d)
-        part_x[k, 1] = far[:, :half]
-        part_y[k, 1] = far[:, half:]
-        give(k, 0, part_x.at[k, 1], got_x.at[k, 1], t_x)
-        give(k, 1, part_y.at[k, 1], got_y.at[k, 1], t_y)
-
-    def down_near(k):
-        near = product(k, t_x)
-        part_x[k, 0] = near[:, :half]
-        held_x[k] = near[:, half:]
-        give(k, 2, part_x.at[k, 0], got_x.at[k, 0], t_x)
-        near = product(k, t_y)
-        part_y[k, 0] = near[:, half:]
-        held_y[k] = near[:, :half]
-        give(k, 3, part_y.at[k, 0], got_y.at[k, 0], t_y)
-
-    def down_own(k):
-        held_own[k] = product(k, t)
-
-    def pass_on(k):
-        arrive(got_x.at[k, 1], rs_send.at[k, 0], rs_recv.at[k, 0])
-        pass_y[k] = (held_y[k].astype(f32) + got_x[k, 1].astype(f32)).astype(bf16)
-        give(k, 4, pass_y.at[k], last_y.at[k], t_y)
-        arrive(got_y.at[k, 1], rs_send.at[k, 1], rs_recv.at[k, 1])
-        pass_x[k] = (held_x[k].astype(f32) + got_y[k, 1].astype(f32)).astype(bf16)
-        give(k, 5, pass_x.at[k], last_x.at[k], t_x)
-
-    def finish(k):
-        arrive(got_x.at[k, 0], rs_send.at[k, 2], rs_recv.at[k, 2])
-        arrive(got_y.at[k, 0], rs_send.at[k, 3], rs_recv.at[k, 3])
-        arrive(last_y.at[k], rs_send.at[k, 4], rs_recv.at[k, 4])
-        arrive(last_x.at[k], rs_send.at[k, 5], rs_recv.at[k, 5])
-        summed[k, :, :half] = (
-            held_own[k, :, :half].astype(f32)
-            + got_x[k, 0].astype(f32) + last_y[k].astype(f32)
-        ).astype(bf16)
-        summed[k, :, half:] = (
-            held_own[k, :, half:].astype(f32)
-            + got_y[k, 0].astype(f32) + last_x[k].astype(f32)
-        ).astype(bf16)
-        if k == 0:
-            send(
-                summed.at[0, rows_of(1 - c, cap), :], ret.at[rows_of(e, cap), :],
-                y_send.at[0], y_recv.at[0], (mate, t),
-            )
-            ret[rows_of(e, cap), :] = summed[0, rows_of(c, cap), :]
-            return
-        for cc in range(2):
-            send(
-                summed.at[k, pl.ds(cc * cap, cap), :], ret.at[rows_of(e, cap), :],
-                y_send.at[2 * k + cc], y_recv.at[2 * k + c], (chip_of(k) * 2 + cc, t),
-            )
+        summed[k, h, :, :half] = low
+        summed[k, h, :, half:] = high
+        send(
+            summed.at[k, h], ret.at[rows_of(e, cap), :],
+            y_send.at[k, h], y_recv.at[k, h], (peer(k, h), t),
+        )
 
     def weighted(first, size):
         at = lax.broadcasted_iota(jnp.int32, (rows, size), 1) + first
@@ -633,14 +649,12 @@
         )
         return one * columns[2, :, 0:1] + two * columns[3, :, 0:1]
 
-    def returned(k):
-        if k == 0:
-            arrive(ret.at[rows_of(mate, cap), :], y_send.at[0], y_recv.at[0])
-        for cc in range(2 if k > 0 else 0):
-            arrive(
-                ret.at[rows_of(chip_of(k) * 2 + cc, cap), :],
-                y_send.at[2 * k + cc], y_recv.at[2 * k + cc],
-            )
+    def returned(k, *part):
+        for h in part or range(2):
+            if k or h:
+                arrive(ret.at[rows_of(peer(k, h), cap), :], y_send.at[k, h], y_recv.at[k, h])
+        if part:
+            return weighted(peer(k, *part) * cap, cap)
         return weighted(chip_of(k) * pair, pair)
 
     taken, chans = gated.shape
@@ -707,36 +721,42 @@
         columns[3] = jnp.broadcast_to(jax.nn.sigmoid(-lead), (128, rows)).T
 
     steps = {
-        "route": routed, "relay": relay, "join": gathered,
-        "up": lambda k: up_half(k, 0, tiles // 2), "more": lambda k: up_half(k, tiles // 2, tiles),
+        "route": route, "relay": relay, "join": join,
+        "up": lambda k, h: up_part(k, h, 0, tiles // 2),
+        "more": lambda k, h: up_part(k, h, tiles // 2, tiles),
         "far": down_far, "near": down_near, "own": down_own,
         "pass": pass_on, "sum": finish, "spread": spread, "conv": convolve, "mix": mixer_end,
     }
 
     def run(plan):
-        back = []
+        left = sum(step.startswith("back") for step in plan)
+        first = True
         for step in plan:
-            name, at = step.rstrip("0123"), [int(step[-1])] if step[-1].isdigit() else []
+            name = step.rstrip("0123")
+            at = [int(digit) for digit in step[len(name):]]
             with jax.named_scope(step):
                 if name != "back":
                     steps[name](*at)
                     continue
-                part = returned(*at)
-                back.append(step)
-                if len(back) == 1:
-                    acc[...] = part
-                elif len(back) < n_z:
-                    acc[...] += part
+                part, left = returned(*at), left - 1
+                total = part if first else acc[...] + part
+                first = False
+                if left:
+                    acc[...] = total
                 else:
-                    out_ref[...] = (acc[...] + part).astype(bf16)
-
-    glu()
-    arrive(xin.at[rows_of(mate, cap), :], z_send.at[0], z_recv.at[0])
-    up_half(0, 0, tiles)
+                    out_ref[...] = total.astype(bf16)
+
+    with jax.named_scope("glu"):
+        glu()
+    with jax.named_scope("mate"):
+        arrive(xin.at[rows_of(mate, cap), :], z_send.at[0, 1], z_recv.at[0, 1])
+    with jax.named_scope("up_own"):
+        up_own()
     load_down.wait()
-    down_far(0)
-    down_near(0)
-    down_own(0)
+    with jax.named_scope("down_own"):
+        down_far(0, 1)
+        down_near(0, 1)
+        down_own(0, 1)
     early = len(sent)
     for side, plan in ((0, outer_plan), (1, inner_plan)):
 
@@ -785,9 +805,9 @@
         shape = array.shape[1:] if array.ndim == 3 else array.shape
         return pltpu.VMEM(shape, array.dtype)
 
-    block = pltpu.VMEM((n_z, pair, half), bf16)
-    blocks = pltpu.VMEM((n_z, 2, pair, half), bf16)
-    wide = pltpu.VMEM((n_z, pair, width), bf16)
+    block = pltpu.VMEM((n_z, 2, cap, half), bf16)
+    blocks = pltpu.VMEM((n_z, 2, 2, cap, half), bf16)
+    wide = pltpu.VMEM((n_z, 2, cap, width), bf16)
     vmem = pl.BlockSpec(memory_space=pltpu.VMEM)
     expert_output, mixer_output = pl.pallas_call(
         functools.partial(paired_kernel, n_ep, n_tp, cap),
@@ -804,20 +824,21 @@
             pltpu.VMEM((cap, feat), bf16),
             pltpu.VMEM((2, cap, feat), bf16),
             pltpu.VMEM((slots, feat), bf16),
-            pltpu.VMEM((n_z, pair, units), bf16),
+            pltpu.VMEM((pair, units), bf16),
+            pltpu.VMEM((n_z - 1, 2, cap, units), bf16),
             blocks, blocks, blocks, blocks, wide, block, block, block, block, block, block,
             wide,
             pltpu.VMEM((slots, width), bf16),
             pltpu.VMEM((rows, width), f32),
             dma((16 + 2 * (units // min(units, 256)),)),
-            dma((n_ep,)),
-            dma((n_ep,)),
-            dma((n_z - 2, 4)),
-            dma((n_z - 2, 4)),
-            dma((n_z, 6)),
-            dma((n_z, 6)),
-            dma((n_ep,)),
-            dma((n_ep,)),
+            dma((n_z, 2)),
+            dma((n_z, 2)),
+            dma((n_z - 2, 2, 4)),
+            dma((n_z - 2, 2, 4)),
+            dma((n_z, 2, 6)),
+            dma((n_z, 2, 6)),
+            dma((n_z, 2)),
+            dma((n_z, 2)),
             pltpu.VMEM((taken, chans), bf16),
             pltpu.VMEM((keep, chans), bf16),
             pltpu.VMEM((keep + taken, chans), f32),

time: 69.8 us -> 66.1 us (0.947)
  the two profiles are of different devices: /device:TPU:1 before, /device:TPU:0 now
where the time goes in v3:
time: 66.1 us; the launch traced here: 65.9 us
  Pallas kernels  62 us (94%)
  local copies, waits for them, and re-layouts  3.24 us (5%)
    pallas_call x1, Pallas kernels, paired_step(): pl.pallas_call(functools.partial(paired_kernel, n_ep, n_tp, cap), out_sha...  62 us
    unnamed x2, local copies, waits for them, and re-layouts  3.24 us

profile of v3, /device:TPU:0, one launch (start us, length us, event | category | flops | bytes accessed | tf_op | source)
XLA Modules:
  0.0 65.9 jit_solution(16264416880601747410)
XLA Ops:
  0.6 62.0 %shard_map.167 = (bf16[256,512]{1,0:T(8,128)(2,1)}, bf16[128,512]{1,0:T(8,128)(2,1)}) custom-call(bf16[256,2048]{1,0:T(8,128)(2,1)} %x_hbm.1, f32[1,2048]{1,0:T(1,128)} %bitcast.9, s32[2,256]{1,0:T(2,128)} %bitcast.11, f32[2,256]{1,0:T(2,128)} %bitcast.12, bf16[1,2048,1024]{2,1,0:T(8,128)(2,1)} %gate_hbm.1, bf16[1,2048,1024]{2,1,0:T(8,128)(2,1)} %up_hbm.1, ...), custom_call_target="tpu_custom_call" | custom-call | flops 9663676416 | bytes 12582912 | tf_op jit(solution)/shard_map/pallas_call | solution.py:812
  62.7 1.6 %copy.20 = bf16[128,512]{1,0:T(8,128)(2,1)} copy(bf16[128,512]{1,0:T(8,128)(2,1)} %get-tuple-element.8) | data formatting | bytes 262144
  64.3 1.7 %copy.21 = bf16[256,512]{1,0:T(8,128)(2,1)} copy(bf16[256,512]{1,0:T(8,128)(2,1)} %get-tuple-element.9) | data formatting | bytes 524288

commit v4 on v3

--- a/solution.py
+++ b/solution.py
@@ -812,8 +812,8 @@
     expert_output, mixer_output = pl.pallas_call(
         functools.partial(paired_kernel, n_ep, n_tp, cap),
         out_shape=(
-            jax.ShapeDtypeStruct((rows, width), bf16),
-            jax.ShapeDtypeStruct((taken, mixer_out_weight.shape[1]), bf16),
+            pltpu.VMEM((rows, width), bf16),
+            pltpu.VMEM((taken, mixer_out_weight.shape[1]), bf16),
         ),
         in_specs=[pl.BlockSpec(memory_space=pltpu.HBM)] * len(operands),
         out_specs=(vmem, vmem),

time: 66.1 us -> 63.5 us (0.961)
  local copies, waits for them, and re-layouts: 3.24 us -> 1.36 us
  Pallas kernels: 62 us -> 61.3 us
    unnamed x2, local copies, waits for them, and re-layouts: 3.24 us -> 1.36 us
    pallas_call x1, Pallas kernels: 62 us -> 61.3 us  [paired_step(): pl.pallas_call(functools.partial(paired_kernel, n_ep, n_tp, cap), out_sha...]
where the time goes in v4:
time: 63.5 us; the launch traced here: 63.3 us
  Pallas kernels  61.3 us (97%)
  local copies, waits for them, and re-layouts  1.36 us (2%)
  between operations  0.65 us (1%)
    pallas_call x1, Pallas kernels, paired_step(): pl.pallas_call(functools.partial(paired_kernel, n_ep, n_tp, cap), out_sha...  61.3 us
    unnamed x2, local copies, waits for them, and re-layouts  1.36 us

profile of v4, /device:TPU:0, one launch (start us, length us, event | category | flops | bytes accessed | tf_op | source)
XLA Modules:
  0.0 63.3 jit_solution(14231165159705640681)
XLA Ops:
  0.6 61.3 %shard_map.167 = (bf16[256,512]{1,0:T(8,128)(2,1)S(1)}, bf16[128,512]{1,0:T(8,128)(2,1)S(1)}) custom-call(bf16[256,2048]{1,0:T(8,128)(2,1)} %x_hbm.1, f32[1,2048]{1,0:T(1,128)} %bitcast.9, s32[2,256]{1,0:T(2,128)} %bitcast.11, f32[2,256]{1,0:T(2,128)} %bitcast.12, bf16[1,2048,1024]{2,1,0:T(8,128)(2,1)} %gate_hbm.1, bf16[1,2048,1024]{2,1,0:T(8,128)(2,1)} %up_hbm.1, ...), custom_call_target="tpu_custom_call" | custom-call | flops 9663676416 | bytes 12582912 | tf_op jit(solution)/shard_map/pallas_call | solution.py:812
  62.0 0.7 %copy.20 = bf16[128,512]{1,0:T(8,128)(2,1)} copy(bf16[128,512]{1,0:T(8,128)(2,1)S(1)} %get-tuple-element.6) | data formatting | bytes 262144
  62.6 0.7 %copy.21 = bf16[256,512]{1,0:T(8,128)(2,1)} copy(bf16[256,512]{1,0:T(8,128)(2,1)S(1)} %get-tuple-element.7) | data formatting | bytes 524288
